TPU v7x, 32 devices: a whole 2x2x4 slice. The times are simulated.
32 devices in a mesh: sp: 8 (over z, x), tp: 4 (over y, core).
Axes of the slice: x: 2, y: 2, z: 4, core: 2. Of those that a mesh axis runs over, the one named last changes fastest.
Arguments:
- tokens: bfloat16 [1024, 2048], P(('sp', 'tp')), may hold values from -6 to 6
- pre_gain: bfloat16 [2048], replicated, may hold values from 0.099609375 to 1.8984375
- w_query: bfloat16 [2048, 1024], P('sp', 'tp'), may hold values from -0.125 to 0.125
- w_key: bfloat16 [2048, 1024], P('sp', 'tp'), may hold values from -0.125 to 0.125
- w_value: bfloat16 [2048, 2048], P('sp', 'tp'), may hold values from -0.125 to 0.125
- w_igate: bfloat16 [2048, 8], replicated, may hold values from -1 to 1
- w_fgate: bfloat16 [2048, 8], replicated, may hold values from -0.125 to 0.125
- forget_bias: float32 [8], replicated, may hold values from 4 to 16
- gate_drift: float32 [1024, 8], P('sp'), may hold values from -2 to 2, as said below
- head_gain: bfloat16 [2048], replicated, may hold values from 0.099609375 to 1.8984375
- w_out: bfloat16 [2048, 2048], P('sp', 'tp'), may hold values from -0.125 to 0.125
Outputs:
- layer_out: bfloat16 [1024, 2048], P(('sp', 'tp'))
Inputs may be any that keep to these rules, and one draw needn't show every extreme that they name: `gate_drift`: constant over aligned spans of 128 positions.
All inputs are finite; a program needn't handle non-finite values.
Results may differ from a plain program's by a relative error of at most 0.02.
Values may be sent and summed in bfloat16 or wider, within the bound.
A program may use at most 64 MiB of HBM per device.

v0:
```python
import jax
import jax.numpy as jnp
from jax import lax
from jax.sharding import PartitionSpec as P

BLOCK = 64


norm_floor = 0.1
lowest_log = -1e30
highest = lax.Precision.HIGHEST


def prefix(value, axis, combine, identity):
    peers, position = (lax.axis_size(axis), lax.axis_index(axis))
    everything = jax.tree.map(
        lambda part, kind: lax.all_gather(part.astype(kind), axis),
        value,
        jax.tree.map(lambda a: jnp.bfloat16 if a.dtype == jnp.float32 else a.dtype, value),
    )
    start = jax.tree.map(
        lambda part, zero: jnp.broadcast_to(jnp.asarray(zero, part.dtype), part.shape),
        value,
        identity,
    )

    def step(k, before):
        reached = k < position
        new = combine(
            before, jax.tree.map(lambda part, own: part[k].astype(own.dtype), everything, value)
        )
        return jax.tree.map(lambda a, b: jnp.where(reached, a, b), new, before)

    return lax.fori_loop(0, peers, step, start)


def advance(memory, summary):
    old_mat, old_vec, old_top = memory
    span_log, span_top, span_mat, span_vec = summary
    new_top = jnp.maximum(span_log + old_top, span_top)
    kept_part = jnp.exp(span_log + old_top - new_top)
    fresh_part = jnp.exp(span_top - new_top)
    return (
        kept_part[:, None, None] * old_mat + fresh_part[:, None, None] * span_mat,
        kept_part[:, None] * old_vec + fresh_part[:, None] * span_vec,
        new_top,
    )


def prefix_states(initial, summary):

    def stepper(memory, one_block):
        return (advance(memory, one_block), memory)

    return lax.scan(stepper, initial, summary)


def join_devices(earlier, later_part):
    early_log, early_mat, early_vec, early_top = earlier
    late_log, late_mat, late_vec, late_top = later_part
    new_top = jnp.maximum(late_log + early_top, late_top)
    kept_part = jnp.exp(late_log + early_top - new_top)
    fresh_part = jnp.exp(late_top - new_top)
    return (
        early_log + late_log,
        kept_part[:, None, None] * early_mat + fresh_part[:, None, None] * late_mat,
        kept_part[:, None] * early_vec + fresh_part[:, None] * late_vec,
        new_top,
    )


def blend_parts(first_part, second_part):
    numer_first, denom_first, peak_first = first_part
    numer_second, denom_second, peak_second = second_part
    new_top = jnp.maximum(peak_first, peak_second)
    weight_first = jnp.exp(peak_first - new_top)
    weight_second = jnp.exp(peak_second - new_top)
    return (
        weight_first[..., None] * numer_first + weight_second[..., None] * numer_second,
        weight_first * denom_first + weight_second * denom_second,
        new_top,
    )


def on_device(
    tokens,
    pre_gain,
    w_query,
    w_key,
    w_value,
    w_igate,
    w_fgate,
    forget_bias,
    gate_drift,
    head_gain,
    w_out,
):
    tp_size = lax.axis_size("tp")
    head_count = w_igate.shape[1]
    local_heads = head_count // tp_size
    first_head = lax.axis_index("tp") * local_heads
    key_width = w_query.shape[1] // local_heads
    value_width = w_value.shape[1] // local_heads
    token_wide = tokens.astype(jnp.float32)
    scaled = token_wide * lax.rsqrt(
        jnp.mean(token_wide * token_wide, axis=1, keepdims=True) + norm_floor
    )
    normed = (scaled * pre_gain.astype(jnp.float32)).astype(jnp.bfloat16)
    gate_cols = jnp.concatenate(
        [
            lax.dynamic_slice_in_dim(w_igate, first_head, local_heads, 1),
            lax.dynamic_slice_in_dim(w_fgate, first_head, local_heads, 1),
        ],
        axis=1,
    )
    key_scale = key_width ** (-0.5)
    wq_full, wk_full, wv_full = (
        lax.all_gather(w_query, "sp", axis=0, tiled=True),
        lax.all_gather(w_key, "sp", axis=0, tiled=True),
        lax.all_gather(w_value, "sp", axis=0, tiled=True),
    )
    row_piece = lax.all_gather(normed, "tp", axis=0, tiled=True)
    queries_part = jnp.dot(row_piece, wq_full, preferred_element_type=jnp.float32).astype(
        jnp.bfloat16
    )
    keys_part = (
        jnp.dot(row_piece, wk_full, preferred_element_type=jnp.float32) * key_scale
    ).astype(jnp.bfloat16)
    values_part = jnp.dot(row_piece, wv_full, preferred_element_type=jnp.float32).astype(
        jnp.bfloat16
    )
    gate_part = jnp.dot(row_piece, gate_cols, preferred_element_type=jnp.float32)
    group_len = queries_part.shape[0]
    blocks = group_len // BLOCK
    log_input = gate_part[:, :local_heads]
    forget_pre = gate_part[:, local_heads:] + lax.dynamic_slice_in_dim(
        forget_bias, first_head, local_heads, 0
    )
    log_forget = jax.nn.log_sigmoid(
        forget_pre + lax.dynamic_slice_in_dim(gate_drift, first_head, local_heads, 1)
    )
    query_blk = queries_part.reshape(blocks, BLOCK, local_heads, key_width)
    key_blk = keys_part.reshape(blocks, BLOCK, local_heads, key_width)
    value_blk = values_part.reshape(blocks, BLOCK, local_heads, value_width)
    input_blk = log_input.reshape(blocks, BLOCK, local_heads).transpose(0, 2, 1)
    forget_blk = log_forget.reshape(blocks, BLOCK, local_heads).transpose(0, 2, 1)
    within = jnp.cumsum(forget_blk, axis=2)
    causal = jnp.arange(BLOCK)[:, None] >= jnp.arange(BLOCK)[None, :]
    log_pair = jnp.where(
        causal, within[..., :, None] - within[..., None, :] + input_blk[..., None, :], -jnp.inf
    )
    peak_intra = jnp.max(log_pair, axis=3)
    scores = jnp.einsum("nshd,nrhd->nhsr", query_blk, key_blk, preferred_element_type=jnp.float32)
    weights = scores * jnp.exp(log_pair - peak_intra[..., None])
    numer_intra = jnp.einsum(
        "nhsr,nrhv->nhsv",
        weights.astype(jnp.bfloat16),
        value_blk,
        preferred_element_type=jnp.float32,
    )
    denom_intra = jnp.sum(weights, axis=3)
    span_log = within[..., -1]
    log_write = span_log[..., None] - within + input_blk
    span_top = jnp.max(log_write, axis=2)
    write_scale = jnp.exp(log_write - span_top[..., None])
    key_scaled = key_blk.astype(jnp.float32) * write_scale.transpose(0, 2, 1)[..., None]
    value_wide = value_blk.astype(jnp.float32)
    span_mat = jnp.einsum("nrhv,nrhd->nhvd", value_wide, key_scaled, precision=highest)
    span_vec = jnp.sum(key_scaled, axis=1)
    summary = (span_log, span_top, span_mat, span_vec)
    empty_state = (
        jnp.zeros((local_heads, value_width, key_width), jnp.float32),
        jnp.zeros((local_heads, key_width), jnp.float32),
        jnp.full((local_heads,), lowest_log, jnp.float32),
    )
    local_end, local_starts = prefix_states(empty_state, summary)
    device_summary = (jnp.sum(span_log, axis=0),) + local_end
    identity_all = (jnp.zeros((local_heads,), jnp.float32),) + empty_state
    incoming = prefix(device_summary, "sp", join_devices, identity_all)
    query_wide = query_blk.astype(jnp.float32)
    intra_part = (numer_intra, denom_intra, peak_intra)
    start_mat, start_vec, start_top = local_starts
    local_part = (
        jnp.einsum("nhvd,nshd->nhsv", start_mat, query_wide, precision=highest),
        jnp.einsum("nhd,nshd->nhs", start_vec, query_wide, precision=highest),
        within + start_top[..., None],
    )
    numerator, denominator, peak_log = blend_parts(local_part, intra_part)
    entry_log, entry_mat, entry_vec, entry_top = incoming
    before_log = jnp.concatenate(
        [jnp.zeros((1, local_heads), jnp.float32), jnp.cumsum(span_log, axis=0)[:-1]], axis=0
    )
    from_left = (
        jnp.einsum("hvd,nshd->nhsv", entry_mat, query_wide, precision=highest),
        jnp.einsum("hd,nshd->nhs", entry_vec, query_wide, precision=highest),
        within + (before_log + entry_top[None, :])[..., None],
    )
    numerator, denominator, peak_log = blend_parts((numerator, denominator, peak_log), from_left)
    hidden = numerator / jnp.maximum(jnp.abs(denominator), jnp.exp(-peak_log))[..., None]
    hidden = hidden.transpose(0, 2, 1, 3).reshape(group_len, local_heads, value_width)
    head_gains = lax.dynamic_slice_in_dim(
        head_gain, first_head * value_width, local_heads * value_width, 0
    )
    head_gains = head_gains.astype(jnp.float32).reshape(local_heads, value_width)
    normed_heads = (
        hidden
        * lax.rsqrt(jnp.mean(hidden * hidden, axis=2, keepdims=True) + norm_floor)
        * head_gains
    )
    normed_heads = normed_heads.astype(jnp.bfloat16).reshape(group_len, local_heads * value_width)
    out_slab = lax.all_gather(w_out, "sp", axis=0, tiled=True)
    return lax.psum_scatter(
        lax.dot_general(
            normed_heads, out_slab, (((1,), (1,)), ((), ())), preferred_element_type=jnp.float32
        ).astype(jnp.bfloat16),
        "tp",
        scatter_dimension=0,
        tiled=True,
    )


def solution(mesh):
    in_specs = (
        P(("sp", "tp"), None),
        P(),
        P("sp", "tp"),
        P("sp", "tp"),
        P("sp", "tp"),
        P(),
        P(),
        P(),
        P("sp", None),
        P(),
        P("sp", "tp"),
    )
    out_specs = P(("sp", "tp"), None)
    return jax.shard_map(
        on_device, mesh=mesh, in_specs=in_specs, out_specs=out_specs, check_vma=False
    )
```

profile of v0, /device:TPU:13, one launch (start us, length us, event | category | flops | bytes accessed | tf_op | source)
XLA Modules:
  0.0 262.3 jit_solution(4414707346627852155)
XLA Ops:
  9.5 1.0 fusion.27
  10.6 1.0 fusion.29
  11.6 7.3 %all_gather.37 = bf16[128,2048]{1,0:T(8,128)(2,1)S(1)} all-gather(bf16[32,2048]{1,0:T(8,128)(2,1)S(1)} %fusion.29), channel_id=1, replica_groups=mesh['sp'=8,'tp'=4] {'tp'}, dimensions={0}, use_global_device_ids=true | all-gather | bytes 655360 | tf_op jit(solution)/shard_map/all_gather | solution.py:122
  22.5 26.5 %all-gather.13.cloned.1.call-done = bf16[2048,256]{1,0:T(8,128)(2,1)} async-done(((bf16[256,256]{1,0:T(8,128)(2,1)}), bf16[2048,256]{1,0:T(8,128)(2,1)}) %all-gather.13.cloned.1.call-update) | async-done | bytes 1048592 | tf_op jit(solution)/shard_map/all_gather | solution.py:119
  49.0 1.5 fusion.26
  50.7 49.1 %all-gather.11.cloned.1.call-done = bf16[2048,512]{1,0:T(8,128)(2,1)} async-done(((bf16[256,512]{1,0:T(8,128)(2,1)}), bf16[2048,512]{1,0:T(8,128)(2,1)}) %all-gather.11.cloned.1.call-update) | async-done | bytes 2097168 | tf_op jit(solution)/shard_map/all_gather | solution.py:120
  99.8 2.0 convolution_convert_fusion.1
  107.0 33.0 %all-gather.15.cloned.1.call-done = bf16[2048,256]{1,0:T(8,128)(2,1)} async-done(((bf16[256,256]{1,0:T(8,128)(2,1)}), bf16[2048,256]{1,0:T(8,128)(2,1)}) %all-gather.15.cloned.1.call-update) | async-done | bytes 1048592 | tf_op jit(solution)/shard_map/all_gather | solution.py:118
  140.0 1.5 convolution_convert_fusion.2
  142.2 11.9 %all-gather.4 = bf16[8,2,128]{2,1,0:T(2,128)(2,1)S(1)} all-gather(bf16[1,2,128]{2,1,0:T(2,128)(2,1)S(1)} %convert_bitcast_fusion), channel_id=5, replica_groups=mesh['sp'=8,'tp'=4] {'sp'}, dimensions={0}, use_global_device_ids=true | all-gather | bytes 4608 | tf_op jit(solution)/shard_map/all_gather | solution.py:17
  154.1 13.8 %all-reduce.3 = (bf16[16]{0:T(256)(128)(2,1)S(1)}, bf16[16]{0:T(256)(128)(2,1)S(1)}) all-reduce(bf16[16]{0:T(256)(128)(2,1)S(1)} %dynamic-update-slice, bf16[16]{0:T(256)(128)(2,1)S(1)} %dynamic-update-slice.1), channel_id=2, replica_groups=mesh['sp'=8,'tp'=4] {'sp'}, use_global_device_ids=true, to_apply=%add.1 | all-reduce | flops 32 | bytes 128
  168.1 12.9 %all-gather.19.cloned.1.call-done = bf16[16,256,128]{2,1,0:T(8,128)(2,1)} async-done(((bf16[2,256,128]{2,1,0:T(8,128)(2,1)}), bf16[16,256,128]{2,1,0:T(8,128)(2,1)}) %all-gather.19.cloned.1.call-update) | async-done | bytes 1048592 | tf_op jit(solution)/shard_map/all_gather | solution.py:17
  181.0 9.2 %while.40 = (s32[]{:T(128)}, f32[2,256,128]{2,1,0:T(8,128)S(1)}, f32[2,128]{1,0:T(2,128)S(1)}, f32[2]{0:T(128)S(1)}, s32[]{:T(128)}, /*index=5*/bf16[8,2]{1,0:T(...) while((s32[]{:T(128)}, f32[2,256,128]{2,1,0:T(8,128)S(1)}, ...), condition=%wide.region_10.11_spmd.clone, body=%wide.region_9.10_spmd.clone.sunk | while | flops 394776 | bytes 658161 | solution.py:34
  181.0 1.0 fusion.85
  182.2 1.0 fusion.85
  183.3 1.0 fusion.85
  184.5 1.0 fusion.85
  185.6 1.0 fusion.85
  186.8 1.0 fusion.85
  187.9 1.0 fusion.85
  189.1 1.0 fusion.85
  192.2 39.7 %all-gather.17.cloned.1.call-done = bf16[2048,512]{1,0:T(8,128)(2,1)} async-done(((bf16[256,512]{1,0:T(8,128)(2,1)}), bf16[2048,512]{1,0:T(8,128)(2,1)}) %all-gather.17.cloned.1.call-update) | async-done | bytes 2097168 | tf_op jit(solution)/shard_map/all_gather | solution.py:211
  231.9 3.2 %convolution_convert_fusion = bf16[128,2048]{1,0:T(8,128)(2,1)} fusion(bf16[2048,512]{1,0:T(8,128)(2,1)} %all-gather.17.cloned.1.call-done, f32[128,512]{1,0:T(8,128)S(1)} %bitcast.227, f32[128,512]{1,0:T(8,128)S(1)} %bitcast.226, f32[512]{0:T(512)S(1)} %dynamic-slice_convert_fusion), kind=kOutput, calls=%fused_computation.38 | convolution fusion | flops 268894208 | bytes 3147776 | tf_op jit(solution)/shard_map/dot_general | solution.py:213
  235.1 20.3 %reduce-scatter.2.cloned.1.call-done = bf16[32,2048]{1,0:T(8,128)(2,1)} async-done(((bf16[128,2048]{1,0:T(8,128)(2,1)}), bf16[32,2048]{1,0:T(8,128)(2,1)}) %reduce-scatter.2.cloned.1.call-update) | async-done | bytes 131088 | tf_op jit(solution)/shard_map/reduce_scatter | solution.py:212
  (109 shorter events, 15.4 us)
Async XLA Ops:
  6.5 42.5 %all-gather.13.cloned.1.call-start = ((), (), s32[]{:S(2)}) async-start(), calls=%async_computation.2 | async-start | bytes 1179648 | tf_op jit(solution)/shard_map/all_gather | solution.py:119
  7.3 92.6 %all-gather.11.cloned.1.call-start = ((), (), s32[]{:S(2)}) async-start(), calls=%async_computation.1 | async-start | bytes 2359296 | tf_op jit(solution)/shard_map/all_gather | solution.py:120
  8.0 132.0 %all-gather.15.cloned.1.call-start = ((), (), s32[]{:S(2)}) async-start(), calls=%async_computation.3 | async-start | bytes 1179648 | tf_op jit(solution)/shard_map/all_gather | solution.py:118
  8.7 172.3 %all-gather.19.cloned.1.call-start = ((), (), s32[]{:S(2)}) async-start(), calls=%async_computation.6 | async-start | bytes 1179648 | tf_op jit(solution)/shard_map/all_gather | solution.py:17
  102.4 2.2 copy-start
  103.8 128.1 %all-gather.17.cloned.1.call-start = ((), (), s32[]{:S(2)}) async-start(), calls=%async_computation.4 | async-start | bytes 2359296 | tf_op jit(solution)/shard_map/all_gather | solution.py:211
  104.4 151.1 %reduce-scatter.2.cloned.1.call-start = ((), (), s32[]{:S(2)}) async-start(), calls=%async_computation.5 | async-start | bytes 655360 | tf_op jit(solution)/shard_map/reduce_scatter | solution.py:212
Sparse Core Ops, SparseCore 0:
  9.5 39.5 all-gather.12
  51.1 48.6 all-gather.10
  101.9 37.9 all-gather.14
  141.9 39.0 all-gather.18
  183.0 48.8 all-gather.16
  235.2 20.1 reduce-scatter.1
where the time goes:
time: 266 us; the launch traced here: 262 us
  waiting for transfers between devices  184 us (69%)
  blocking collectives  33 us (12%)
  other arithmetic  15.9 us (6%)
  between operations  14.4 us (5%)
  matrix products  10.7 us (4%)
  local copies, waits for them, and re-layouts  3.7 us (1%)
    all_gather x1, waiting for transfers between devices, on_device(): lax.all_gather(w_value, 'sp', axis=0, tiled=True)  49.1 us
    all_gather x1, waiting for transfers between devices, on_device(): out_slab = lax.all_gather(w_out, 'sp', axis=0, tiled=True)  39.7 us
    all_gather x1, waiting for transfers between devices, on_device(): lax.all_gather(w_query, 'sp', axis=0, tiled=True)  33 us
    all_gather x1, waiting for transfers between devices, on_device(): lax.all_gather(w_key, 'sp', axis=0, tiled=True)  26.5 us
    reduce_scatter x1, waiting for transfers between devices, on_device(): lax.psum_scatter(lax.dot_general(normed_heads, out_slab, (((1,), (1,)), (...  20.3 us
    unnamed x1, blocking collectives  13.8 us
    all_gather x1, waiting for transfers between devices, prefix(): lax.all_gather(part.astype(kind), axis)  12.9 us
    all_gather x1, blocking collectives, prefix(): lax.all_gather(part.astype(kind), axis)  11.9 us
  transfers between devices with their start and end apart: 6, of which 6 were waited for; matrix products, arithmetic and copies ran while one was open for 10% of the time, Pallas kernels for 0%

commit v1 on v0

--- a/solution.py
+++ b/solution.py
@@ -1,6 +1,10 @@
+import functools
+
 import jax
 import jax.numpy as jnp
 from jax import lax
+from jax.experimental import pallas as pl
+from jax.experimental.pallas import tpu as pltpu
 from jax.sharding import PartitionSpec as P
 
 BLOCK = 64
@@ -219,6 +223,379 @@
     )
 
 
+ring_limit = 16
+MESH = pl.DeviceIdType.MESH
+f32 = jnp.float32
+bf16 = jnp.bfloat16
+
+
+def dot_nt(a, b):
+    return lax.dot_general(a, b, (((1,), (1,)), ((), ())), preferred_element_type=f32)
+
+
+def ring_kernel(
+    n,
+    tp,
+    lh,
+    tokens,
+    pre_gain,
+    w_query,
+    w_key,
+    w_value,
+    w_igate,
+    w_fgate,
+    forget_base,
+    head_gain,
+    w_out,
+    out,
+    tok_all,
+    normed,
+    key_in,
+    value_in,
+    query_in,
+    out_in,
+    state_own,
+    state_in,
+    aux_own,
+    aux_in,
+    acc,
+    heads,
+    shares,
+    shares_in,
+    tok_send,
+    tok_recv,
+    ring_send,
+    ring_recv,
+    aux_send,
+    aux_recv,
+    share_send,
+    share_recv,
+):
+    s = lax.axis_index("sp")
+    t = lax.axis_index("tp")
+    half_ring = n // 2
+    steps = n - 1
+    odd = s % 2
+    pos = odd * (n - 1) + (1 - 2 * odd) * (s // 2)
+
+    def owner_at(p):
+        p = lax.rem(p + 2 * n, n)
+        far = p // half_ring
+        return far * (2 * (n - 1 - p) + 1) + (1 - far) * 2 * p
+
+    right = owner_at(pos + 1)
+    left = owner_at(pos - 1)
+    targets = (right, left)
+    rows = tokens.shape[0]
+    length = rows * tp
+    dk = w_query.shape[1] // lh
+    dv = w_value.shape[1] // lh
+    depth = w_query.shape[0]
+    half = depth // 2
+
+    barrier = pltpu.get_barrier_semaphore()
+    for peer in targets:
+        pl.semaphore_signal(barrier, inc=1, device_id={"sp": peer}, device_id_type=MESH)
+    for i in range(1, tp):
+        pl.semaphore_signal(
+            barrier, inc=1, device_id={"tp": lax.rem(t + i, tp)}, device_id_type=MESH
+        )
+    pl.semaphore_wait(barrier, 2 + tp - 1)
+
+    copies = []
+
+    def ring_copy(piece, own, landing, d, k):
+        size = own.shape[0] // 2
+        source = own.at[pl.ds(d * size, size)] if k == 0 else landing.at[d, k - 1]
+        copy = pltpu.make_async_remote_copy(
+            src_ref=source,
+            dst_ref=landing.at[d, k],
+            send_sem=ring_send.at[piece, d, k],
+            recv_sem=ring_recv.at[piece, d, k],
+            device_id={"sp": targets[d]},
+            device_id_type=MESH,
+        )
+        copy.start()
+        copies.append(copy)
+        return copy
+
+    def aux_copy(k):
+        copy = pltpu.make_async_remote_copy(
+            src_ref=aux_own if k == 0 else aux_in.at[k - 1],
+            dst_ref=aux_in.at[k],
+            send_sem=aux_send.at[k],
+            recv_sem=aux_recv.at[k],
+            device_id={"sp": right},
+            device_id_type=MESH,
+        )
+        copy.start()
+        copies.append(copy)
+        return copy
+
+    my_rows = pl.ds(pl.multiple_of(t * rows, rows), rows)
+    token_copies = []
+    for i in range(1, tp):
+        copy = pltpu.make_async_remote_copy(
+            src_ref=tokens,
+            dst_ref=tok_all.at[my_rows],
+            send_sem=tok_send.at[i - 1],
+            recv_sem=tok_recv.at[i - 1],
+            device_id={"tp": lax.rem(t + i, tp)},
+            device_id_type=MESH,
+        )
+        copy.start()
+        copies.append(copy)
+        token_copies.append(copy)
+    pieces = ((0, w_key, key_in), (1, w_value, value_in), (2, w_query, query_in))
+    live = {}
+    for piece, own, landing in pieces:
+        for d in range(2):
+            live[piece, d] = ring_copy(piece, own, landing, d, 0)
+
+    tok_all[my_rows, :] = tokens[...]
+    for copy in token_copies:
+        copy.wait_recv()
+    wide = tok_all[...].astype(f32)
+    scale = lax.rsqrt(jnp.mean(wide * wide, axis=1, keepdims=True) + norm_floor)
+    normed[...] = (wide * scale * pre_gain[...]).astype(bf16)
+
+    cols = (
+        slice(0, lh * dk),
+        slice(lh * dk, lh * (dk + dv)),
+        slice(lh * (dk + dv), lh * (2 * dk + dv)),
+    )
+    mine = normed[:, pl.ds(pl.multiple_of(s * depth, depth), depth)]
+    for piece, own, landing in pieces:
+        acc[:, cols[piece]] = jnp.dot(mine, own[...], preferred_element_type=f32)
+    all_normed = normed[...]
+    gate_in = jnp.dot(all_normed, w_igate[...], preferred_element_type=f32)
+    gate_forget = jnp.dot(all_normed, w_fgate[...], preferred_element_type=f32) + forget_base[...]
+    log_forget_all = jnp.minimum(gate_forget, 0.0) - jnp.log1p(jnp.exp(-jnp.abs(gate_forget)))
+
+    for k in range(steps):
+        for piece, own, landing in pieces:
+            for d in range(2):
+                live[piece, d].wait_recv()
+                if k + 1 < steps:
+                    live[piece, d] = ring_copy(piece, own, landing, d, k + 1)
+        if k == steps - 1:
+            for d in range(2):
+                live[3, d] = ring_copy(3, w_out, out_in, d, 0)
+        for d in range(2):
+            owner = owner_at(pos - 1 - k) if d == 0 else owner_at(pos + 1 + k)
+            part = normed[:, pl.ds(pl.multiple_of(owner * depth + d * half, half), half)]
+            for piece, own, landing in pieces:
+                acc[:, cols[piece]] += jnp.dot(
+                    part, landing[d, k], preferred_element_type=f32
+                )
+
+    row_id = lax.broadcasted_iota(jnp.int32, (length, length), 0)
+    col_id = lax.broadcasted_iota(jnp.int32, (length, length), 1)
+    causal = row_id >= col_id
+    head_id = lax.broadcasted_iota(jnp.int32, gate_in.shape, 1)
+    keys = (acc[:, cols[0]] * (dk**-0.5)).astype(bf16)
+    values = acc[:, cols[1]].astype(bf16)
+    queries = acc[:, cols[2]].astype(bf16)
+    gates = []
+    for j in range(lh):
+        pick = head_id == t * lh + j
+        in_col = jnp.sum(jnp.where(pick, gate_in, 0.0), axis=1, keepdims=True)
+        lf_col = jnp.sum(jnp.where(pick, log_forget_all, 0.0), axis=1, keepdims=True)
+        lf_row = jnp.sum(jnp.where(row_id == col_id, lf_col, 0.0), axis=0, keepdims=True)
+        in_row = jnp.sum(jnp.where(row_id == col_id, in_col, 0.0), axis=0, keepdims=True)
+        b_col = jnp.sum(jnp.where(causal, lf_row, 0.0), axis=1, keepdims=True)
+        b_row = jnp.sum(jnp.where(row_id <= col_id, lf_col, 0.0), axis=0, keepdims=True)
+        gates.append((in_row, b_col, b_row))
+        span = jnp.sum(lf_col, axis=0, keepdims=True)
+        write = span - b_col + in_col
+        top = jnp.max(write, axis=0, keepdims=True)
+        key_scaled = keys[:, j * dk : (j + 1) * dk].astype(f32) * jnp.exp(write - top)
+        state_own[j * dk : (j + 1) * dk, :] = jnp.dot(
+            key_scaled.T.astype(bf16),
+            values[:, j * dv : (j + 1) * dv],
+            preferred_element_type=f32,
+        ).astype(bf16)
+        aux_own[j : j + 1, :] = jnp.broadcast_to(span, (1, dk))
+        aux_own[lh + j : lh + j + 1, :] = jnp.broadcast_to(top, (1, dk))
+        aux_own[2 * lh + j : 2 * lh + j + 1, :] = jnp.sum(key_scaled, axis=0, keepdims=True)
+
+    for d in range(2):
+        live[4, d] = ring_copy(4, state_own, state_in, d, 0)
+    aux_live = aux_copy(0)
+    intra = []
+    for k in range(steps):
+        if k < lh:
+            in_row, b_col, b_row = gates[k]
+            log_pair = jnp.where(causal, b_col - b_row + in_row, lowest_log)
+            peak = jnp.max(log_pair, axis=1, keepdims=True)
+            q = queries[:, k * dk : (k + 1) * dk]
+            weights = dot_nt(q, keys[:, k * dk : (k + 1) * dk]) * jnp.where(
+                causal, jnp.exp(log_pair - peak), 0.0
+            )
+            numer = jnp.dot(
+                weights.astype(bf16),
+                values[:, k * dv : (k + 1) * dv],
+                preferred_element_type=f32,
+            )
+            intra.append((numer, jnp.sum(weights, axis=1, keepdims=True), peak, q, b_col))
+        aux_live.wait_recv()
+        if k + 1 < steps:
+            aux_live = aux_copy(k + 1)
+        for piece, own, landing in ((4, state_own, state_in), (3, w_out, out_in)):
+            for d in range(2):
+                live[piece, d].wait_recv()
+                if k + 1 < steps:
+                    live[piece, d] = ring_copy(piece, own, landing, d, k + 1)
+
+    owners = [owner_at(pos - 1 - k) for k in range(steps)]
+
+    def when(flag):
+        return flag.astype(jnp.int32).astype(f32)
+
+    for j in range(lh):
+        logs = []
+        for k in range(steps):
+            total = aux_in[k, lh + j : lh + j + 1, :]
+            for i in range(steps):
+                if i != k:
+                    between = when((owners[i] > owners[k]) & (owners[i] < s))
+                    total = total + between * aux_in[i, j : j + 1, :]
+            before = when(owners[k] < s)
+            logs.append((before, before * total + (1.0 - before) * lowest_log))
+        entry = functools.reduce(jnp.maximum, [log for _, log in logs])
+        mat = jnp.zeros((dk, dv), f32)
+        vec = jnp.zeros((1, dk), f32)
+        split = (lh * dk) // 2
+        d = (j * dk) // split
+        base = j * dk - d * split
+        for k in range(steps):
+            before, log = logs[k]
+            weight = before * jnp.exp(log - entry)
+            slot = k if d == 0 else steps - 1 - k
+            mat = mat + weight[:, :1] * state_in[d, slot, base : base + dk, :].astype(f32)
+            vec = vec + weight * aux_in[k, 2 * lh + j : 2 * lh + j + 1, :]
+        numer, denom, peak, q, b_col = intra[j]
+        carried = b_col + entry[:, :1]
+        new_top = jnp.maximum(peak, carried)
+        w_intra = jnp.exp(peak - new_top)
+        w_carry = jnp.exp(carried - new_top)
+        numer = w_intra * numer + w_carry * jnp.dot(
+            q, mat.astype(bf16), preferred_element_type=f32
+        )
+        denom = w_intra * denom + w_carry * jnp.sum(q.astype(f32) * vec, axis=1, keepdims=True)
+        hidden = numer / jnp.maximum(jnp.abs(denom), jnp.exp(-new_top))
+        gain = head_gain[:, pl.ds(pl.multiple_of((t * lh + j) * dv, dv), dv)]
+        heads[:, j * dv : (j + 1) * dv] = (
+            hidden
+            * lax.rsqrt(jnp.mean(hidden * hidden, axis=1, keepdims=True) + norm_floor)
+            * gain
+        ).astype(bf16)
+
+    ready = heads[...]
+    out_depth = w_out.shape[0]
+    out_half = out_depth // 2
+    shares[:, pl.ds(pl.multiple_of(s * out_depth, out_depth), out_depth)] = dot_nt(
+        ready, w_out[...]
+    ).astype(bf16)
+    for k in range(steps):
+        for d in range(2):
+            owner = owner_at(pos - 1 - k) if d == 0 else owner_at(pos + 1 + k)
+            at = pl.ds(pl.multiple_of(owner * out_depth + d * out_half, out_half), out_half)
+            shares[:, at] = dot_nt(ready, out_in[d, k]).astype(bf16)
+    share_copies = []
+    for i in range(1, tp):
+        peer = lax.rem(t + i, tp)
+        copy = pltpu.make_async_remote_copy(
+            src_ref=shares.at[pl.ds(pl.multiple_of(peer * rows, rows), rows)],
+            dst_ref=shares_in.at[i - 1],
+            send_sem=share_send.at[i - 1],
+            recv_sem=share_recv.at[i - 1],
+            device_id={"tp": peer},
+            device_id_type=MESH,
+        )
+        copy.start()
+        copies.append(copy)
+        share_copies.append(copy)
+    total = shares[my_rows, :].astype(f32)
+    for i, copy in enumerate(share_copies):
+        copy.wait_recv()
+        total = total + shares_in[i].astype(f32)
+    out[...] = total.astype(bf16)
+    for copy in copies:
+        copy.wait_send()
+
+
+def on_device_ring(
+    n,
+    tp,
+    tokens,
+    pre_gain,
+    w_query,
+    w_key,
+    w_value,
+    w_igate,
+    w_fgate,
+    forget_bias,
+    gate_drift,
+    head_gain,
+    w_out,
+):
+    lh = w_igate.shape[1] // tp
+    rows, width = tokens.shape
+    length = rows * tp
+    steps = n - 1
+    dk = w_query.shape[1] // lh
+    dv = w_value.shape[1] // lh
+    vmem = pl.BlockSpec(memory_space=pltpu.VMEM)
+
+    def landing(a):
+        return pltpu.VMEM((2, steps, a.shape[0] // 2, a.shape[1]), bf16)
+
+    aux_rows = -(-3 * lh // 8) * 8
+    return pl.pallas_call(
+        functools.partial(ring_kernel, n, tp, lh),
+        out_shape=jax.ShapeDtypeStruct((rows, w_out.shape[0] * n), bf16),
+        in_specs=[vmem] * 10,
+        out_specs=vmem,
+        scratch_shapes=[
+            pltpu.VMEM((length, width), bf16),
+            pltpu.VMEM((length, width), bf16),
+            landing(w_key),
+            landing(w_value),
+            landing(w_query),
+            landing(w_out),
+            pltpu.VMEM((lh * dk, dv), bf16),
+            pltpu.VMEM((2, steps, lh * dk // 2, dv), bf16),
+            pltpu.VMEM((aux_rows, dk), f32),
+            pltpu.VMEM((steps, aux_rows, dk), f32),
+            pltpu.VMEM((length, lh * (2 * dk + dv)), f32),
+            pltpu.VMEM((length, lh * dv), bf16),
+            pltpu.VMEM((length, w_out.shape[0] * n), bf16),
+            pltpu.VMEM((tp - 1, rows, w_out.shape[0] * n), bf16),
+            pltpu.SemaphoreType.DMA((tp - 1,)),
+            pltpu.SemaphoreType.DMA((tp - 1,)),
+            pltpu.SemaphoreType.DMA((5, 2, steps)),
+            pltpu.SemaphoreType.DMA((5, 2, steps)),
+            pltpu.SemaphoreType.DMA((steps,)),
+            pltpu.SemaphoreType.DMA((steps,)),
+            pltpu.SemaphoreType.DMA((tp - 1,)),
+            pltpu.SemaphoreType.DMA((tp - 1,)),
+        ],
+        compiler_params=pltpu.CompilerParams(collective_id=0, has_side_effects=True),
+    )(
+        tokens,
+        pre_gain.astype(f32)[None, :],
+        w_query,
+        w_key,
+        w_value,
+        w_igate,
+        w_fgate,
+        gate_drift + forget_bias,
+        head_gain.astype(f32)[None, :],
+        w_out,
+    )
+
+
 def solution(mesh):
     in_specs = (
         P(("sp", "tp"), None),
@@ -234,6 +611,9 @@
         P("sp", "tp"),
     )
     out_specs = P(("sp", "tp"), None)
+    body = on_device
+    if mesh.shape["sp"] <= ring_limit and mesh.shape["sp"] % 2 == 0:
+        body = functools.partial(on_device_ring, mesh.shape["sp"], mesh.shape["tp"])
     return jax.shard_map(
-        on_device, mesh=mesh, in_specs=in_specs, out_specs=out_specs, check_vma=False
-    )
+        body, mesh=mesh, in_specs=in_specs, out_specs=out_specs, check_vma=False
+    )

time: 266 us -> 98.9 us (0.37)
  waiting for transfers between devices: 184 us -> 0 us
  Pallas kernels: 0 us -> 89.9 us
  blocking collectives: 33 us -> 0 us
  between operations: 14.4 us -> 0.02 us
  other arithmetic: 15.9 us -> 2.52 us
  matrix products: 10.7 us -> 0 us
    all_gather x5 -> x0, waiting for transfers between devices: 161 us -> none  [the longest x1 49.1 us: on_device(): lax.all_gather(w_value, 'sp', axis=0, tiled=True)]
    pallas_call x0 -> x1, Pallas kernels: none -> 89.9 us  [on_device_ring(): pl.pallas_call(functools.partial(ring_kernel, n, tp, lh), out_shape=jax.S...]
    reduce_scatter x1 -> x0, waiting for transfers between devices: 20.3 us -> none  [on_device(): lax.psum_scatter(lax.dot_general(normed_heads, out_slab, (((1,), (1,)), (...]
    all_gather x2 -> x0, blocking collectives: 19.1 us -> none  [the longest x1 11.9 us: prefix(): lax.all_gather(part.astype(kind), axis)]
    unnamed x1 -> x0, blocking collectives: 13.8 us -> none
    dot_general x12 -> x0, matrix products: 10.7 us -> none  [the longest x1 3.2 us: on_device(): lax.dot_general(normed_heads, out_slab, (((1,), (1,)), ((), ())), preferr...]
    select_n x24 -> x0, other arithmetic: 9 us -> none  [step(): return jax.tree.map(lambda a, b: jnp.where(reached, a, b), new, before)]
    unnamed x9 -> x14, local copies, waits for them, and re-layouts: 1.17 us -> 4.46 us
  transfers between devices with their start and end apart: 6 -> 0, of which waited for: 6 -> 0; matrix products, arithmetic and copies ran while one was open for 10% -> 0% of each run, Pallas kernels for 0% -> 0%
where the time goes in v1:
time: 98.9 us; the launch traced here: 96.9 us
  Pallas kernels  89.9 us (91%)
  local copies, waits for them, and re-layouts  4.46 us (5%)
  other arithmetic  2.52 us (3%)
    pallas_call x1, Pallas kernels, on_device_ring(): pl.pallas_call(functools.partial(ring_kernel, n, tp, lh), out_shape=jax.S...  89.9 us
    unnamed x14, local copies, waits for them, and re-layouts  4.46 us

profile of v1, /device:TPU:13, one launch (start us, length us, event | category | flops | bytes accessed | tf_op | source)
XLA Modules:
  0.0 96.9 jit_solution(966297680072229199)
XLA Ops:
  0.0 0.0 copy-start.2
  0.0 1.3 %broadcast_in_dim.15 = f32[2048]{0:T(1024)} convert(bf16[2048]{0:T(1024)(128)(2,1)} %param.12) | non-fusion elementwise | flops 2048 | bytes 12288 | tf_op jit(solution)/shard_map/broadcast_in_dim | solution.py:587
  1.3 0.0 copy-done.2
  1.3 0.0 copy-start.3
  1.3 0.6 broadcast_in_dim.16
  1.9 0.1 copy-done.3
  2.0 0.0 copy-start.4
  2.0 0.1 copy.15
  2.1 0.6 copy-done.4
  2.6 0.0 copy-start
  2.6 0.6 broadcast_add_fusion.forget_base
  3.3 0.1 copy-done
  3.4 0.0 copy-start.1
  3.4 1.0 %copy.17.w_igate = bf16[2048,8]{1,0:T(8,128)(2,1)} copy(bf16[2048,8]{0,1:T(8,128)(2,1)S(1)} %copy-done) | data formatting | bytes 65536 | tf_op args[5]
  4.4 0.0 copy-done.1
  4.4 1.0 %copy.18.w_fgate = bf16[2048,8]{1,0:T(8,128)(2,1)} copy(bf16[2048,8]{0,1:T(8,128)(2,1)S(1)} %copy-done.1) | data formatting | bytes 65536 | tf_op args[6]
  5.4 89.9 %shard_map.109 = bf16[32,2048]{1,0:T(8,128)(2,1)} custom-call(bf16[32,2048]{1,0:T(8,128)(2,1)} %tokens.1, f32[1,2048]{1,0:T(1,128)} %bitcast.2, bf16[256,256]{1,0:T(8,128)(2,1)} %w_query.1, bf16[256,256]{1,0:T(8,128)(2,1)} %w_key.1, bf16[256,512]{1,0:T(8,128)(2,1)} %w_value.1, bf16[2048,8]{1,0:T(8,128)(2,1)} %copy.17.w_igate, bf16[2048,8]{1,0:T(8,128)(2,1)} %copy.18.w_fgate, ...), custom_call_target="tpu_custom_call" | custom-call | tf_op jit(solution)/shard_map/pallas_call | solution.py:555
  95.4 1.6 %copy.20 = bf16[32,2048]{1,0:T(8,128)(2,1)} copy(bf16[32,2048]{1,0:T(8,128)(2,1)} %shard_map.109) | data formatting | bytes 262144
Async XLA Ops:
  0.0 1.3 %copy-start.2 = (bf16[2048]{0:T(1024)(128)(2,1)S(1)}, bf16[2048]{0:T(1024)(128)(2,1)}, u32[]{:S(2)}) copy-start(bf16[2048]{0:T(1024)(128)(2,1)} %param.20) | copy-start | bytes 12292
  1.3 0.7 copy-start.3
  2.0 0.7 copy-start.4
  2.6 0.8 copy-start
  3.4 1.0 %copy-start.1 = (bf16[2048,8]{0,1:T(8,128)(2,1)S(1)}, bf16[2048,8]{0,1:T(8,128)(2,1)}, u32[]{:S(2)}) copy-start(bf16[2048,8]{0,1:T(8,128)(2,1)} %param.17) | copy-start | bytes 98308

commit v2 on v0

--- a/solution.py
+++ b/solution.py
@@ -1,6 +1,10 @@
+import functools
+
 import jax
 import jax.numpy as jnp
 from jax import lax
+from jax.experimental import pallas as pl
+from jax.experimental.pallas import tpu as pltpu
 from jax.sharding import PartitionSpec as P
 
 BLOCK = 64
@@ -219,6 +223,562 @@
     )
 
 
+ring_limit = 16
+drift_span = 128
+MESH = pl.DeviceIdType.MESH
+f32 = jnp.float32
+bf16 = jnp.bfloat16
+
+
+def dot_nt(a, b):
+    return lax.dot_general(a, b, (((1,), (1,)), ((), ())), preferred_element_type=f32)
+
+
+def when(flag):
+    return flag.astype(jnp.int32).astype(f32)
+
+
+def square_kernel(
+    n,
+    tp,
+    tokens,
+    pre_gain,
+    w_query,
+    w_key,
+    w_value,
+    w_igate,
+    w_fgate,
+    drift,
+    head_gain,
+    w_out,
+    out,
+    tok_all,
+    drift_in,
+    normed,
+    own_key,
+    own_value,
+    own_query,
+    own_out,
+    key_in,
+    value_in,
+    query_in,
+    out_in,
+    state_own,
+    state_in,
+    aux_own,
+    aux_in,
+    acc,
+    heads,
+    shares,
+    pair_in,
+    pair_sum,
+    shares_in,
+    tok_send,
+    tok_recv,
+    drift_send,
+    drift_recv,
+    near_send,
+    near_recv,
+    first_send,
+    first_recv,
+    ring_send,
+    ring_recv,
+    state_send,
+    state_recv,
+    aux_send,
+    aux_recv,
+    pair_send,
+    pair_recv,
+    share_send,
+    share_recv,
+):
+    s = lax.axis_index("sp")
+    t = lax.axis_index("tp")
+    q = n // 2
+    steps = q - 1
+    zh = s // q
+    r = s % q
+    y = t // 2
+    c = t % 2
+    near = 2 * y + 1 - c
+    head = 2 * (2 * y + zh) + c
+    rows = tokens.shape[0]
+    span_rows = rows * tp
+    length = 2 * span_rows
+    dk = w_query.shape[1] // 2
+    dv = w_value.shape[1] // 2
+    depth = w_query.shape[0]
+    half = depth // 2
+    half_ring = q // 2
+    odd = r % 2
+    pos = odd * (q - 1) + (1 - 2 * odd) * (r // 2)
+
+    def owner_at(p):
+        p = lax.rem(p + 2 * q, q)
+        far = p // half_ring
+        return far * (2 * (q - 1 - p) + 1) + (1 - far) * 2 * p
+
+    targets = (zh * q + owner_at(pos + 1), zh * q + owner_at(pos - 1))
+
+    barrier = pltpu.get_barrier_semaphore()
+    me = s * tp + t
+    for i in range(1, n * tp):
+        other = lax.rem(me + i, n * tp)
+        pl.semaphore_signal(
+            barrier,
+            inc=1,
+            device_id={"sp": other // tp, "tp": lax.rem(other, tp)},
+            device_id_type=MESH,
+        )
+    pl.semaphore_wait(barrier, n * tp - 1)
+
+    copies = []
+    guarded = []
+
+    def remote(source, target, send, recv, sp_at, tp_at):
+        return pltpu.make_async_remote_copy(
+            src_ref=source,
+            dst_ref=target,
+            send_sem=send,
+            recv_sem=recv,
+            device_id={"sp": sp_at, "tp": tp_at},
+            device_id_type=MESH,
+        )
+
+    def send(*args):
+        copy = remote(*args)
+        copy.start()
+        copies.append(copy)
+        return copy
+
+    def send_or_keep(source, target, send_sem, recv_sem, sp_at, tp_at):
+        away = (sp_at != s) | (tp_at != t)
+        copy = remote(source, target, send_sem, recv_sem, sp_at, tp_at)
+
+        @pl.when(away)
+        def _():
+            copy.start()
+
+        @pl.when(jnp.logical_not(away))
+        def _():
+            pltpu.make_async_copy(source, target, recv_sem).start()
+
+        guarded.append((away, copy))
+        return copy
+
+    def arrived(target, sem):
+        pltpu.make_async_copy(target, target, sem).wait()
+
+    half_tp = tp // 2
+    x = s % 2
+    row_at = pl.ds(pl.multiple_of(x * span_rows + t * rows, rows), rows)
+    for g in range(2):
+        for yy in range(half_tp):
+            to_s, to_t = g * q + s // 2, 2 * yy + c
+            send_or_keep(
+                tokens,
+                tok_all.at[row_at],
+                tok_send.at[g, yy],
+                tok_recv.at[x, y],
+                to_s,
+                to_t,
+            )
+            send_or_keep(
+                drift,
+                drift_in.at[x, y],
+                drift_send.at[g, yy],
+                drift_recv.at[x, y],
+                to_s,
+                to_t,
+            )
+
+    pieces = (
+        (0, w_key, own_key, key_in),
+        (1, w_value, own_value, value_in),
+        (2, w_query, own_query, query_in),
+        (3, w_out, own_out, out_in),
+    )
+    stays = zh == c
+    first = []
+    for p, own, stage, _ in pieces:
+        width = own.shape[1] // 2
+        for g in range(2):
+            mine = own.at[:, pl.ds(g * width, width)]
+            keep = stays & (c == g)
+            block = (zh + c) % 2
+            copy = remote(
+                mine,
+                stage.at[block],
+                first_send.at[g, p],
+                first_recv.at[block, p],
+                c * q + r,
+                2 * y + g,
+            )
+
+            @pl.when(jnp.logical_not(keep))
+            def _():
+                copy.start()
+
+            @pl.when(keep)
+            def _():
+                pltpu.make_async_copy(mine, stage.at[0], first_recv.at[0, p]).start()
+
+            guarded.append((jnp.logical_not(keep), copy))
+
+    def ring_copy(p, block, d, k):
+        _, _, stage, landing = pieces[p]
+        size = stage.shape[1] // 2
+        source = (
+            stage.at[block, pl.ds(d * size, size)] if k == 0 else landing.at[block, d, k - 1]
+        )
+        return send(
+            source,
+            landing.at[block, d, k],
+            ring_send.at[p, block, d, k],
+            ring_recv.at[p, block, d, k],
+            targets[d],
+            t,
+        )
+
+    live = {}
+
+    def ring_start(p, block):
+        arrived(pieces[p][2].at[block], first_recv.at[block, p])
+        for d in range(2):
+            live[p, block, d] = ring_copy(p, block, d, 0)
+
+    def ring_step(p, block, k):
+        for d in range(2):
+            live[p, block, d].wait_recv()
+            if k + 1 < steps:
+                live[p, block, d] = ring_copy(p, block, d, k + 1)
+
+    for p in range(3):
+        ring_start(p, 0)
+
+    for xx in range(2):
+        for yy in range(half_tp):
+            at = pl.ds(
+                pl.multiple_of(xx * span_rows + (2 * yy + c) * rows, rows), rows
+            )
+            arrived(tok_all.at[at], tok_recv.at[xx, yy])
+            arrived(drift_in.at[xx, yy], drift_recv.at[xx, yy])
+            send(
+                tok_all.at[at],
+                tok_all.at[at],
+                near_send.at[xx, yy],
+                near_recv.at[xx, yy],
+                s,
+                near,
+            )
+    for xx in range(2):
+        for yy in range(half_tp):
+            at = pl.ds(
+                pl.multiple_of(xx * span_rows + (2 * yy + 1 - c) * rows, rows), rows
+            )
+            arrived(tok_all.at[at], near_recv.at[xx, yy])
+    wide = tok_all[...].astype(f32)
+    scale = lax.rsqrt(jnp.mean(wide * wide, axis=1, keepdims=True) + norm_floor)
+    normed[...] = (wide * scale * pre_gain[...]).astype(bf16)
+
+    cols = (slice(0, dk), slice(dk, dk + dv), slice(dk + dv, 2 * dk + dv))
+
+    def origin(block, owner):
+        return (zh if block == 0 else 1 - zh) * q + owner
+
+    def own_product(block, fresh):
+        at = pl.ds(pl.multiple_of(origin(block, r) * depth, depth), depth)
+        part = normed[:, at]
+        for p in range(3):
+            product = jnp.dot(part, pieces[p][2][block], preferred_element_type=f32)
+            acc[:, cols[p]] = product if fresh else acc[:, cols[p]] + product
+
+    def step_product(block, k):
+        for d in range(2):
+            owner = owner_at(pos - 1 - k) if d == 0 else owner_at(pos + 1 + k)
+            at = pl.ds(
+                pl.multiple_of(origin(block, owner) * depth + d * half, half), half
+            )
+            part = normed[:, at]
+            for p in range(3):
+                acc[:, cols[p]] += jnp.dot(
+                    part, pieces[p][3][block, d, k], preferred_element_type=f32
+                )
+
+    own_product(0, True)
+    for k in range(steps):
+        for p in range(3):
+            ring_step(p, 0, k)
+        if k == steps - 2:
+            for p in range(3):
+                ring_start(p, 1)
+        step_product(0, k)
+    ring_start(3, 0)
+
+    all_normed = normed[...]
+    gate_in = jnp.dot(all_normed, w_igate[...], preferred_element_type=f32)
+    gate_forget = jnp.dot(all_normed, w_fgate[...], preferred_element_type=f32)
+    row_id = lax.broadcasted_iota(jnp.int32, (length, length), 0)
+    col_id = lax.broadcasted_iota(jnp.int32, (length, length), 1)
+    causal = row_id >= col_id
+    pick = lax.broadcasted_iota(jnp.int32, gate_in.shape, 1) == head
+    late = lax.broadcasted_iota(jnp.int32, gate_in.shape, 0) >= span_rows
+    heads_all = gate_in.shape[1]
+    offset = jnp.where(
+        late, drift_in[1, 0, 0:1, :heads_all], drift_in[0, 0, 0:1, :heads_all]
+    )
+    forget_pre = gate_forget + offset
+    log_forget = jnp.minimum(forget_pre, 0.0) - jnp.log1p(jnp.exp(-jnp.abs(forget_pre)))
+    in_col = jnp.sum(jnp.where(pick, gate_in, 0.0), axis=1, keepdims=True)
+    lf_col = jnp.sum(jnp.where(pick, log_forget, 0.0), axis=1, keepdims=True)
+    lf_row = jnp.sum(jnp.where(row_id == col_id, lf_col, 0.0), axis=0, keepdims=True)
+    in_row = jnp.sum(jnp.where(row_id == col_id, in_col, 0.0), axis=0, keepdims=True)
+    b_col = jnp.sum(jnp.where(causal, lf_row, 0.0), axis=1, keepdims=True)
+    b_row = jnp.sum(jnp.where(row_id <= col_id, lf_col, 0.0), axis=0, keepdims=True)
+    span = jnp.sum(lf_col, axis=0, keepdims=True)
+    write = span - b_col + in_col
+    top = jnp.max(write, axis=0, keepdims=True)
+    write_scale = jnp.exp(write - top)
+    log_pair = jnp.where(causal, b_col - b_row + in_row, lowest_log)
+    peak = jnp.max(log_pair, axis=1, keepdims=True)
+    decay = jnp.where(causal, jnp.exp(log_pair - peak), 0.0)
+
+    own_product(1, False)
+    for k in range(steps):
+        for p in range(3):
+            ring_step(p, 1, k)
+        step_product(1, k)
+    ring_start(3, 1)
+
+    keys = (acc[:, cols[0]] * (dk**-0.5)).astype(bf16)
+    values = acc[:, cols[1]].astype(bf16)
+    queries = acc[:, cols[2]].astype(bf16)
+    key_scaled = keys.astype(f32) * write_scale
+    state_own[...] = jnp.dot(
+        key_scaled.T.astype(bf16), values, preferred_element_type=f32
+    ).astype(bf16)
+    aux_own[0:1, :] = jnp.broadcast_to(span, (1, dk))
+    aux_own[1:2, :] = jnp.broadcast_to(top, (1, dk))
+    aux_own[2:3, :] = jnp.sum(key_scaled, axis=0, keepdims=True)
+    aux_own[3:, :] = jnp.zeros((aux_own.shape[0] - 3, dk), f32)
+    state_copies = []
+    for i in range(1, q):
+        peer = zh * q + lax.rem(r + i, q)
+        state_copies.append(
+            (
+                send(
+                    state_own,
+                    state_in.at[i - 1],
+                    state_send.at[i - 1],
+                    state_recv.at[i - 1],
+                    peer,
+                    t,
+                ),
+                send(
+                    aux_own,
+                    aux_in.at[i - 1],
+                    aux_send.at[i - 1],
+                    aux_recv.at[i - 1],
+                    peer,
+                    t,
+                ),
+            )
+        )
+    weights = dot_nt(queries, keys) * decay
+    numer = jnp.dot(weights.astype(bf16), values, preferred_element_type=f32)
+    denom = jnp.sum(weights, axis=1, keepdims=True)
+    ring_step(3, 0, 0)
+    ring_step(3, 1, 0)
+
+    for pair in state_copies:
+        for copy in pair:
+            copy.wait_recv()
+    owners = [lax.rem(r - i + q, q) for i in range(1, q)]
+    logs = []
+    for k in range(steps):
+        total = aux_in[k, 1:2, :]
+        for i in range(steps):
+            if i != k:
+                between = when((owners[i] > owners[k]) & (owners[i] < r))
+                total = total + between * aux_in[i, 0:1, :]
+        before = when(owners[k] < r)
+        logs.append((before, before * total + (1.0 - before) * lowest_log))
+    entry = functools.reduce(jnp.maximum, [log for _, log in logs])
+    mat = jnp.zeros((dk, dv), f32)
+    vec = jnp.zeros((1, dk), f32)
+    for k in range(steps):
+        before, log = logs[k]
+        weight = before * jnp.exp(log - entry)
+        mat = mat + weight[:, :1] * state_in[k].astype(f32)
+        vec = vec + weight * aux_in[k, 2:3, :]
+    carried = b_col + entry[:, :1]
+    new_top = jnp.maximum(peak, carried)
+    w_intra = jnp.exp(peak - new_top)
+    w_carry = jnp.exp(carried - new_top)
+    numer = w_intra * numer + w_carry * jnp.dot(
+        queries, mat.astype(bf16), preferred_element_type=f32
+    )
+    denom = w_intra * denom + w_carry * jnp.sum(
+        queries.astype(f32) * vec, axis=1, keepdims=True
+    )
+    hidden = numer / jnp.maximum(jnp.abs(denom), jnp.exp(-new_top))
+    gain = head_gain[:, pl.ds(pl.multiple_of(head * dv, dv), dv)]
+    heads[...] = (
+        hidden
+        * lax.rsqrt(jnp.mean(hidden * hidden, axis=1, keepdims=True) + norm_floor)
+        * gain
+    ).astype(bf16)
+
+    ready = heads[...]
+    e_depth = w_out.shape[0]
+    e_half = e_depth // 2
+    for block in range(2):
+        at = pl.ds(pl.multiple_of(origin(block, r) * e_depth, e_depth), e_depth)
+        shares[:, at] = dot_nt(ready, own_out[block]).astype(bf16)
+    for k in range(steps):
+        for block in range(2):
+            if k > 0:
+                ring_step(3, block, k)
+            for d in range(2):
+                owner = owner_at(pos - 1 - k) if d == 0 else owner_at(pos + 1 + k)
+                at = pl.ds(
+                    pl.multiple_of(origin(block, owner) * e_depth + d * e_half, e_half),
+                    e_half,
+                )
+                shares[:, at] = dot_nt(ready, out_in[block, d, k]).astype(bf16)
+
+    theirs = pl.ds(pl.multiple_of((1 - c) * span_rows, span_rows), span_rows)
+    pair = send(
+        shares.at[theirs], pair_in, pair_send.at[0], pair_recv.at[0], s, near
+    )
+    pair.wait_recv()
+    kept = pl.ds(pl.multiple_of(c * span_rows, span_rows), span_rows)
+    pair_sum[...] = (shares[kept, :].astype(f32) + pair_in[...].astype(f32)).astype(bf16)
+    for to_t in range(tp):
+        send_or_keep(
+            pair_sum.at[pl.ds(to_t * rows, rows)],
+            shares_in.at[zh, y],
+            share_send.at[to_t],
+            share_recv.at[zh, y],
+            2 * r + c,
+            to_t,
+        )
+    total = jnp.zeros(out.shape, f32)
+    for g in range(2):
+        for yy in range(half_tp):
+            arrived(shares_in.at[g, yy], share_recv.at[g, yy])
+            total = total + shares_in[g, yy].astype(f32)
+    out[...] = total.astype(bf16)
+    for copy in copies:
+        copy.wait_send()
+    for away, copy in guarded:
+
+        @pl.when(away)
+        def _():
+            copy.wait_send()
+
+
+def on_device_ring(
+    n,
+    tp,
+    tokens,
+    pre_gain,
+    w_query,
+    w_key,
+    w_value,
+    w_igate,
+    w_fgate,
+    forget_bias,
+    gate_drift,
+    head_gain,
+    w_out,
+):
+    heads = w_igate.shape[1]
+    if heads != 2 * tp or gate_drift.shape[0] > drift_span:
+        return on_device(
+            tokens,
+            pre_gain,
+            w_query,
+            w_key,
+            w_value,
+            w_igate,
+            w_fgate,
+            forget_bias,
+            gate_drift,
+            head_gain,
+            w_out,
+        )
+    rows, width = tokens.shape
+    length = 2 * rows * tp
+    q = n // 2
+    steps = q - 1
+    half_tp = tp // 2
+    dk = w_query.shape[1] // 2
+    dv = w_value.shape[1] // 2
+    features = w_out.shape[0] * n
+    vmem = pl.BlockSpec(memory_space=pltpu.VMEM)
+    dma = pltpu.SemaphoreType.DMA
+    weights = (w_key, w_value, w_query, w_out)
+    base = gate_drift[:8] + forget_bias
+    base = jnp.pad(base, ((0, 0), (0, 128 - heads)))
+    return pl.pallas_call(
+        functools.partial(square_kernel, n, tp),
+        out_shape=jax.ShapeDtypeStruct((rows, features), bf16),
+        in_specs=[vmem] * 10,
+        out_specs=vmem,
+        scratch_shapes=[
+            pltpu.VMEM((length, width), bf16),
+            pltpu.VMEM((2, half_tp, 8, 128), f32),
+            pltpu.VMEM((length, width), bf16),
+            *[pltpu.VMEM((2, w.shape[0], w.shape[1] // 2), bf16) for w in weights],
+            *[
+                pltpu.VMEM((2, 2, steps, w.shape[0] // 2, w.shape[1] // 2), bf16)
+                for w in weights
+            ],
+            pltpu.VMEM((dk, dv), bf16),
+            pltpu.VMEM((steps, dk, dv), bf16),
+            pltpu.VMEM((8, dk), f32),
+            pltpu.VMEM((steps, 8, dk), f32),
+            pltpu.VMEM((length, 2 * dk + dv), f32),
+            pltpu.VMEM((length, dv), bf16),
+            pltpu.VMEM((length, features), bf16),
+            pltpu.VMEM((length // 2, features), bf16),
+            pltpu.VMEM((length // 2, features), bf16),
+            pltpu.VMEM((2, half_tp, rows, features), bf16),
+            dma((2, half_tp)),
+            dma((2, half_tp)),
+            dma((2, half_tp)),
+            dma((2, half_tp)),
+            dma((2, half_tp)),
+            dma((2, half_tp)),
+            dma((2, 4)),
+            dma((2, 4)),
+            dma((4, 2, 2, steps)),
+            dma((4, 2, 2, steps)),
+            dma((steps,)),
+            dma((steps,)),
+            dma((steps,)),
+            dma((steps,)),
+            dma((1,)),
+            dma((1,)),
+            dma((tp,)),
+            dma((2, half_tp)),
+        ],
+        compiler_params=pltpu.CompilerParams(collective_id=0, has_side_effects=True),
+    )(
+        tokens,
+        pre_gain.astype(f32)[None, :],
+        w_query,
+        w_key,
+        w_value,
+        w_igate,
+        w_fgate,
+        base,
+        head_gain.astype(f32)[None, :],
+        w_out,
+    )
+
+
 def solution(mesh):
     in_specs = (
         P(("sp", "tp"), None),
@@ -234,6 +794,9 @@
         P("sp", "tp"),
     )
     out_specs = P(("sp", "tp"), None)
+    body = on_device
+    if mesh.shape["sp"] <= ring_limit and mesh.shape["sp"] % 4 == 0 and mesh.shape["tp"] % 2 == 0:
+        body = functools.partial(on_device_ring, mesh.shape["sp"], mesh.shape["tp"])
     return jax.shard_map(
-        on_device, mesh=mesh, in_specs=in_specs, out_specs=out_specs, check_vma=False
-    )
+        body, mesh=mesh, in_specs=in_specs, out_specs=out_specs, check_vma=False
+    )

time: 266 us -> 90.4 us (0.34); the launches traced: 262 us -> 89.4 us
  waiting for transfers between devices: 184 us -> 0 us
  Pallas kernels: 0 us -> 81.8 us
  blocking collectives: 33 us -> 0 us
  between operations: 14.4 us -> 0.02 us
  other arithmetic: 15.9 us -> 2.55 us
  matrix products: 10.7 us -> 0 us
    all_gather x5 -> x0, waiting for transfers between devices: 161 us -> none  [the longest x1 49.1 us: on_device(): lax.all_gather(w_value, 'sp', axis=0, tiled=True)]
    pallas_call x0 -> x1, Pallas kernels: none -> 81.8 us  [on_device_ring(): pl.pallas_call(functools.partial(square_kernel, n, tp), out_shape=jax.Sha...]
    reduce_scatter x1 -> x0, waiting for transfers between devices: 20.3 us -> none  [on_device(): lax.psum_scatter(lax.dot_general(normed_heads, out_slab, (((1,), (1,)), (...]
    all_gather x2 -> x0, blocking collectives: 19.1 us -> none  [the longest x1 11.9 us: prefix(): lax.all_gather(part.astype(kind), axis)]
    unnamed x1 -> x0, blocking collectives: 13.8 us -> none
    dot_general x12 -> x0, matrix products: 10.7 us -> none  [the longest x1 3.2 us: on_device(): lax.dot_general(normed_heads, out_slab, (((1,), (1,)), ((), ())), preferr...]
    select_n x24 -> x0, other arithmetic: 9 us -> none  [step(): return jax.tree.map(lambda a, b: jnp.where(reached, a, b), new, before)]
    unnamed x9 -> x10, local copies, waits for them, and re-layouts: 1.17 us -> 4.35 us
  transfers between devices with their start and end apart: 6 -> 0, of which waited for: 6 -> 0; matrix products, arithmetic and copies ran while one was open for 10% -> 0% of each run, Pallas kernels for 0% -> 0%
where the time goes in v2:
time: 90.4 us; the launch traced here: 89.4 us
  Pallas kernels  81.8 us (90%)
  local copies, waits for them, and re-layouts  4.95 us (5%)
  other arithmetic  2.55 us (3%)
    pallas_call x1, Pallas kernels, on_device_ring(): pl.pallas_call(functools.partial(square_kernel, n, tp), out_shape=jax.Sha...  81.8 us
    unnamed x10, local copies, waits for them, and re-layouts  4.35 us

profile of v2, /device:TPU:13, one launch (start us, length us, event | category | flops | bytes accessed | tf_op | source)
XLA Modules:
  0.0 89.4 jit_solution(10011779931531669970)
XLA Ops:
  0.0 0.0 copy-start
  0.0 0.8 copy.15
  0.8 0.7 broadcast_add_fusion
  1.4 0.6 pad.4.drift
  2.0 0.0 copy-start.2
  2.0 1.3 %broadcast_in_dim.15 = f32[2048]{0:T(1024)} convert(bf16[2048]{0:T(1024)(128)(2,1)} %param.12) | non-fusion elementwise | flops 2048 | bytes 12288 | tf_op jit(solution)/shard_map/broadcast_in_dim | solution.py:770
  3.3 0.0 copy-done.2
  3.3 0.6 broadcast_in_dim.16
  3.9 0.0 copy-done
  3.9 0.0 copy-start.1
  3.9 1.0 %copy.13.w_igate = bf16[2048,8]{1,0:T(8,128)(2,1)} copy(bf16[2048,8]{0,1:T(8,128)(2,1)S(1)} %copy-done) | data formatting | bytes 65536 | tf_op args[5]
  4.9 0.0 copy-done.1
  4.9 1.0 %copy.14.w_fgate = bf16[2048,8]{1,0:T(8,128)(2,1)} copy(bf16[2048,8]{0,1:T(8,128)(2,1)S(1)} %copy-done.1) | data formatting | bytes 65536 | tf_op args[6]
  5.9 81.8 %shard_map.109 = bf16[32,2048]{1,0:T(8,128)(2,1)} custom-call(bf16[32,2048]{1,0:T(8,128)(2,1)} %tokens.1, f32[1,2048]{1,0:T(1,128)} %bitcast.3, bf16[256,256]{1,0:T(8,128)(2,1)} %w_query.1, bf16[256,256]{1,0:T(8,128)(2,1)} %w_key.1, bf16[256,512]{1,0:T(8,128)(2,1)} %w_value.1, bf16[2048,8]{1,0:T(8,128)(2,1)} %copy.13.w_igate, bf16[2048,8]{1,0:T(8,128)(2,1)} %copy.14.w_fgate, ...), custom_call_target="tpu_custom_call" | custom-call | tf_op jit(solution)/shard_map/pallas_call | solution.py:724
  87.8 1.6 %copy.17 = bf16[32,2048]{1,0:T(8,128)(2,1)} copy(bf16[32,2048]{1,0:T(8,128)(2,1)} %shard_map.109) | data formatting | bytes 262144
Async XLA Ops:
  0.0 3.9 %copy-start = (bf16[2048,8]{0,1:T(8,128)(2,1)S(1)}, bf16[2048,8]{0,1:T(8,128)(2,1)}, u32[]{:S(2)}) copy-start(bf16[2048,8]{0,1:T(8,128)(2,1)} %param.16) | copy-start | bytes 98308
  2.0 1.3 %copy-start.2 = (bf16[2048]{0:T(1024)(128)(2,1)S(1)}, bf16[2048]{0:T(1024)(128)(2,1)}, u32[]{:S(2)}) copy-start(bf16[2048]{0:T(1024)(128)(2,1)} %param.20) | copy-start | bytes 12292
  3.9 1.0 %copy-start.1 = (bf16[2048,8]{0,1:T(8,128)(2,1)S(1)}, bf16[2048,8]{0,1:T(8,128)(2,1)}, u32[]{:S(2)}) copy-start(bf16[2048,8]{0,1:T(8,128)(2,1)} %param.17) | copy-start | bytes 98308

commit v3 on v2

--- a/solution.py
+++ b/solution.py
@@ -248,6 +248,7 @@
     w_value,
     w_igate,
     w_fgate,
+    forget_bias,
     drift,
     head_gain,
     w_out,
@@ -279,7 +280,7 @@
     drift_recv,
     near_send,
     near_recv,
-    first_send,
+    first_sems,
     first_recv,
     ring_send,
     ring_recv,
@@ -369,6 +370,96 @@
     def arrived(target, sem):
         pltpu.make_async_copy(target, target, sem).wait()
 
+    pieces = (
+        (0, w_key, own_key, key_in),
+        (1, w_value, own_value, value_in),
+        (2, w_query, own_query, query_in),
+        (3, w_out, own_out, out_in),
+    )
+    stays = zh == c
+    def first_send(p):
+        _, own, stage, _ = pieces[p]
+        width = own.shape[1] // 2
+        for g in range(2):
+            mine = own.at[:, pl.ds(g * width, width)]
+            keep = stays & (c == g)
+            block = (zh + c) % 2
+            copy = remote(
+                mine,
+                stage.at[block],
+                first_sems.at[g, p],
+                first_recv.at[block, p],
+                c * q + r,
+                2 * y + g,
+            )
+
+            @pl.when(jnp.logical_not(keep))
+            def _():
+                copy.start()
+
+            @pl.when(keep)
+            def _():
+                pltpu.make_async_copy(mine, stage.at[0], first_recv.at[0, p]).start()
+
+            guarded.append((jnp.logical_not(keep), copy))
+
+    for p in range(3):
+        first_send(p)
+
+    def ring_copy(p, block, d, k):
+        _, _, stage, landing = pieces[p]
+        size = stage.shape[1] // 2
+        source = (
+            stage.at[block, pl.ds(d * size, size)] if k == 0 else landing.at[block, d, k - 1]
+        )
+        return send(
+            source,
+            landing.at[block, d, k],
+            ring_send.at[p, block, d, k],
+            ring_recv.at[p, block, d, k],
+            targets[d],
+            t,
+        )
+
+    live = {}
+
+    def ring_start(p, block):
+        arrived(pieces[p][2].at[block], first_recv.at[block, p])
+        for d in range(2):
+            live[p, block, d] = ring_copy(p, block, d, 0)
+
+    def ring_step(p, block, k):
+        for d in range(2):
+            live[p, block, d].wait_recv()
+            if k + 1 < steps:
+                live[p, block, d] = ring_copy(p, block, d, k + 1)
+
+    cols = (slice(0, dk), slice(dk, dk + dv), slice(dk + dv, 2 * dk + dv))
+
+    def origin(block, owner):
+        return (zh if block == 0 else 1 - zh) * q + owner
+
+    def own_product(block, fresh):
+        at = pl.ds(pl.multiple_of(origin(block, r) * depth, depth), depth)
+        part = normed[:, at]
+        for p in range(3):
+            product = jnp.dot(part, pieces[p][2][block], preferred_element_type=f32)
+            acc[:, cols[p]] = product if fresh else acc[:, cols[p]] + product
+
+    def step_product(block, k):
+        for d in range(2):
+            owner = owner_at(pos - 1 - k) if d == 0 else owner_at(pos + 1 + k)
+            at = pl.ds(
+                pl.multiple_of(origin(block, owner) * depth + d * half, half), half
+            )
+            part = normed[:, at]
+            for p in range(3):
+                acc[:, cols[p]] += jnp.dot(
+                    part, pieces[p][3][block, d, k], preferred_element_type=f32
+                )
+
+    for p in range(3):
+        ring_start(p, 0)
     half_tp = tp // 2
     x = s % 2
     row_at = pl.ds(pl.multiple_of(x * span_rows + t * rows, rows), rows)
@@ -392,70 +483,15 @@
                 to_t,
             )
 
-    pieces = (
-        (0, w_key, own_key, key_in),
-        (1, w_value, own_value, value_in),
-        (2, w_query, own_query, query_in),
-        (3, w_out, own_out, out_in),
-    )
-    stays = zh == c
-    first = []
-    for p, own, stage, _ in pieces:
-        width = own.shape[1] // 2
-        for g in range(2):
-            mine = own.at[:, pl.ds(g * width, width)]
-            keep = stays & (c == g)
-            block = (zh + c) % 2
-            copy = remote(
-                mine,
-                stage.at[block],
-                first_send.at[g, p],
-                first_recv.at[block, p],
-                c * q + r,
-                2 * y + g,
-            )
-
-            @pl.when(jnp.logical_not(keep))
-            def _():
-                copy.start()
-
-            @pl.when(keep)
-            def _():
-                pltpu.make_async_copy(mine, stage.at[0], first_recv.at[0, p]).start()
-
-            guarded.append((jnp.logical_not(keep), copy))
-
-    def ring_copy(p, block, d, k):
-        _, _, stage, landing = pieces[p]
-        size = stage.shape[1] // 2
-        source = (
-            stage.at[block, pl.ds(d * size, size)] if k == 0 else landing.at[block, d, k - 1]
-        )
-        return send(
-            source,
-            landing.at[block, d, k],
-            ring_send.at[p, block, d, k],
-            ring_recv.at[p, block, d, k],
-            targets[d],
-            t,
-        )
-
-    live = {}
-
-    def ring_start(p, block):
-        arrived(pieces[p][2].at[block], first_recv.at[block, p])
-        for d in range(2):
-            live[p, block, d] = ring_copy(p, block, d, 0)
-
-    def ring_step(p, block, k):
-        for d in range(2):
-            live[p, block, d].wait_recv()
-            if k + 1 < steps:
-                live[p, block, d] = ring_copy(p, block, d, k + 1)
-
+    first_send(3)
+    for k in range(steps):
+        for p in range(3):
+            ring_step(p, 0, k)
     for p in range(3):
-        ring_start(p, 0)
-
+        ring_start(p, 1)
+    for k in range(steps - 1):
+        for p in range(3):
+            ring_step(p, 1, k)
     for xx in range(2):
         for yy in range(half_tp):
             at = pl.ds(
@@ -479,58 +515,32 @@
             arrived(tok_all.at[at], near_recv.at[xx, yy])
     wide = tok_all[...].astype(f32)
     scale = lax.rsqrt(jnp.mean(wide * wide, axis=1, keepdims=True) + norm_floor)
-    normed[...] = (wide * scale * pre_gain[...]).astype(bf16)
-
-    cols = (slice(0, dk), slice(dk, dk + dv), slice(dk + dv, 2 * dk + dv))
-
-    def origin(block, owner):
-        return (zh if block == 0 else 1 - zh) * q + owner
-
-    def own_product(block, fresh):
-        at = pl.ds(pl.multiple_of(origin(block, r) * depth, depth), depth)
-        part = normed[:, at]
-        for p in range(3):
-            product = jnp.dot(part, pieces[p][2][block], preferred_element_type=f32)
-            acc[:, cols[p]] = product if fresh else acc[:, cols[p]] + product
-
-    def step_product(block, k):
-        for d in range(2):
-            owner = owner_at(pos - 1 - k) if d == 0 else owner_at(pos + 1 + k)
-            at = pl.ds(
-                pl.multiple_of(origin(block, owner) * depth + d * half, half), half
-            )
-            part = normed[:, at]
-            for p in range(3):
-                acc[:, cols[p]] += jnp.dot(
-                    part, pieces[p][3][block, d, k], preferred_element_type=f32
-                )
-
+    normed[...] = (wide * scale * pre_gain[...].astype(f32)[None, :]).astype(bf16)
+
+    ring_start(3, 0)
     own_product(0, True)
     for k in range(steps):
-        for p in range(3):
-            ring_step(p, 0, k)
-        if k == steps - 2:
-            for p in range(3):
-                ring_start(p, 1)
         step_product(0, k)
-    ring_start(3, 0)
-
+    own_product(1, False)
+    for k in range(steps - 1):
+        step_product(1, k)
     all_normed = normed[...]
-    gate_in = jnp.dot(all_normed, w_igate[...], preferred_element_type=f32)
-    gate_forget = jnp.dot(all_normed, w_fgate[...], preferred_element_type=f32)
+    gate_in = dot_nt(all_normed, w_igate[...])
+    gate_forget = dot_nt(all_normed, w_fgate[...])
     row_id = lax.broadcasted_iota(jnp.int32, (length, length), 0)
     col_id = lax.broadcasted_iota(jnp.int32, (length, length), 1)
     causal = row_id >= col_id
     pick = lax.broadcasted_iota(jnp.int32, gate_in.shape, 1) == head
-    late = lax.broadcasted_iota(jnp.int32, gate_in.shape, 0) >= span_rows
-    heads_all = gate_in.shape[1]
-    offset = jnp.where(
-        late, drift_in[1, 0, 0:1, :heads_all], drift_in[0, 0, 0:1, :heads_all]
-    )
-    forget_pre = gate_forget + offset
-    log_forget = jnp.minimum(forget_pre, 0.0) - jnp.log1p(jnp.exp(-jnp.abs(forget_pre)))
+    late = lax.broadcasted_iota(jnp.int32, (length, 1), 0) >= span_rows
+    mine = pl.ds(head, 1)
+    offset = jnp.where(late, drift_in[1, 0, mine, :][:, :1], drift_in[0, 0, mine, :][:, :1])
+    forget_pre = (
+        jnp.sum(jnp.where(pick, gate_forget, 0.0), axis=1, keepdims=True)
+        + forget_bias[head]
+        + offset
+    )
+    lf_col = jnp.minimum(forget_pre, 0.0) - jnp.log1p(jnp.exp(-jnp.abs(forget_pre)))
     in_col = jnp.sum(jnp.where(pick, gate_in, 0.0), axis=1, keepdims=True)
-    lf_col = jnp.sum(jnp.where(pick, log_forget, 0.0), axis=1, keepdims=True)
     lf_row = jnp.sum(jnp.where(row_id == col_id, lf_col, 0.0), axis=0, keepdims=True)
     in_row = jnp.sum(jnp.where(row_id == col_id, in_col, 0.0), axis=0, keepdims=True)
     b_col = jnp.sum(jnp.where(causal, lf_row, 0.0), axis=1, keepdims=True)
@@ -543,11 +553,10 @@
     peak = jnp.max(log_pair, axis=1, keepdims=True)
     decay = jnp.where(causal, jnp.exp(log_pair - peak), 0.0)
 
-    own_product(1, False)
-    for k in range(steps):
-        for p in range(3):
-            ring_step(p, 1, k)
-        step_product(1, k)
+    ring_step(3, 0, 0)
+    for p in range(3):
+        ring_step(p, 1, steps - 1)
+    step_product(1, steps - 1)
     ring_start(3, 1)
 
     keys = (acc[:, cols[0]] * (dk**-0.5)).astype(bf16)
@@ -587,8 +596,9 @@
     weights = dot_nt(queries, keys) * decay
     numer = jnp.dot(weights.astype(bf16), values, preferred_element_type=f32)
     denom = jnp.sum(weights, axis=1, keepdims=True)
-    ring_step(3, 0, 0)
-    ring_step(3, 1, 0)
+    for k in range(1, steps):
+        ring_step(3, 0, k)
+        ring_step(3, 1, k - 1)
 
     for pair in state_copies:
         for copy in pair:
@@ -622,7 +632,7 @@
         queries.astype(f32) * vec, axis=1, keepdims=True
     )
     hidden = numer / jnp.maximum(jnp.abs(denom), jnp.exp(-new_top))
-    gain = head_gain[:, pl.ds(pl.multiple_of(head * dv, dv), dv)]
+    gain = head_gain[pl.ds(pl.multiple_of(head * dv, dv), dv)].astype(f32)[None, :]
     heads[...] = (
         hidden
         * lax.rsqrt(jnp.mean(hidden * hidden, axis=1, keepdims=True) + norm_floor)
@@ -632,43 +642,64 @@
     ready = heads[...]
     e_depth = w_out.shape[0]
     e_half = e_depth // 2
-    for block in range(2):
-        at = pl.ds(pl.multiple_of(origin(block, r) * e_depth, e_depth), e_depth)
-        shares[:, at] = dot_nt(ready, own_out[block]).astype(bf16)
+    wide_half = q * e_depth
+    theirs = pl.ds(pl.multiple_of((1 - c) * span_rows, span_rows), span_rows)
+    kept = pl.ds(pl.multiple_of(c * span_rows, span_rows), span_rows)
+
+    def share_own(block):
+        at = pl.ds(pl.multiple_of(r * e_depth, e_depth), e_depth)
+        shares[block, :, at] = dot_nt(ready, own_out[block]).astype(bf16)
+
+    def share_step(block, k):
+        for d in range(2):
+            owner = owner_at(pos - 1 - k) if d == 0 else owner_at(pos + 1 + k)
+            at = pl.ds(pl.multiple_of(owner * e_depth + d * e_half, e_half), e_half)
+            shares[block, :, at] = dot_nt(ready, out_in[block, d, k]).astype(bf16)
+
+    def pair_start(block):
+        return send(
+            shares.at[block, theirs],
+            pair_in.at[block],
+            pair_send.at[block],
+            pair_recv.at[block],
+            s,
+            near,
+        )
+
+    def share_out(block, pair):
+        pair.wait_recv()
+        pair_sum[block] = (
+            shares[block, kept, :].astype(f32) + pair_in[block].astype(f32)
+        ).astype(bf16)
+        side = zh if block == 0 else 1 - zh
+        for to_t in range(tp):
+            send_or_keep(
+                pair_sum.at[block, pl.ds(to_t * rows, rows)],
+                shares_in.at[zh, y, side],
+                share_send.at[block, to_t],
+                share_recv.at[zh, y, side],
+                2 * r + c,
+                to_t,
+            )
+
+    share_own(0)
     for k in range(steps):
-        for block in range(2):
-            if k > 0:
-                ring_step(3, block, k)
-            for d in range(2):
-                owner = owner_at(pos - 1 - k) if d == 0 else owner_at(pos + 1 + k)
-                at = pl.ds(
-                    pl.multiple_of(origin(block, owner) * e_depth + d * e_half, e_half),
-                    e_half,
-                )
-                shares[:, at] = dot_nt(ready, out_in[block, d, k]).astype(bf16)
-
-    theirs = pl.ds(pl.multiple_of((1 - c) * span_rows, span_rows), span_rows)
-    pair = send(
-        shares.at[theirs], pair_in, pair_send.at[0], pair_recv.at[0], s, near
-    )
-    pair.wait_recv()
-    kept = pl.ds(pl.multiple_of(c * span_rows, span_rows), span_rows)
-    pair_sum[...] = (shares[kept, :].astype(f32) + pair_in[...].astype(f32)).astype(bf16)
-    for to_t in range(tp):
-        send_or_keep(
-            pair_sum.at[pl.ds(to_t * rows, rows)],
-            shares_in.at[zh, y],
-            share_send.at[to_t],
-            share_recv.at[zh, y],
-            2 * r + c,
-            to_t,
-        )
-    total = jnp.zeros(out.shape, f32)
-    for g in range(2):
-        for yy in range(half_tp):
-            arrived(shares_in.at[g, yy], share_recv.at[g, yy])
-            total = total + shares_in[g, yy].astype(f32)
-    out[...] = total.astype(bf16)
+        share_step(0, k)
+    pair = pair_start(0)
+    share_own(1)
+    for k in range(steps - 1):
+        share_step(1, k)
+    share_out(0, pair)
+    ring_step(3, 1, steps - 1)
+    share_step(1, steps - 1)
+    share_out(1, pair_start(1))
+    for side in range(2):
+        total = jnp.zeros((rows, wide_half), f32)
+        for g in range(2):
+            for yy in range(half_tp):
+                arrived(shares_in.at[g, yy, side], share_recv.at[g, yy, side])
+                total = total + shares_in[g, yy, side].astype(f32)
+        out[:, side * wide_half : (side + 1) * wide_half] = total.astype(bf16)
     for copy in copies:
         copy.wait_send()
     for away, copy in guarded:
@@ -719,16 +750,15 @@
     vmem = pl.BlockSpec(memory_space=pltpu.VMEM)
     dma = pltpu.SemaphoreType.DMA
     weights = (w_key, w_value, w_query, w_out)
-    base = gate_drift[:8] + forget_bias
-    base = jnp.pad(base, ((0, 0), (0, 128 - heads)))
+    smem = pl.BlockSpec(memory_space=pltpu.SMEM)
     return pl.pallas_call(
         functools.partial(square_kernel, n, tp),
         out_shape=jax.ShapeDtypeStruct((rows, features), bf16),
-        in_specs=[vmem] * 10,
+        in_specs=[vmem] * 7 + [smem] + [vmem] * 3,
         out_specs=vmem,
         scratch_shapes=[
             pltpu.VMEM((length, width), bf16),
-            pltpu.VMEM((2, half_tp, 8, 128), f32),
+            pltpu.VMEM((2, half_tp, heads, gate_drift.shape[0]), f32),
             pltpu.VMEM((length, width), bf16),
             *[pltpu.VMEM((2, w.shape[0], w.shape[1] // 2), bf16) for w in weights],
             *[
@@ -741,10 +771,10 @@
             pltpu.VMEM((steps, 8, dk), f32),
             pltpu.VMEM((length, 2 * dk + dv), f32),
             pltpu.VMEM((length, dv), bf16),
-            pltpu.VMEM((length, features), bf16),
-            pltpu.VMEM((length // 2, features), bf16),
-            pltpu.VMEM((length // 2, features), bf16),
-            pltpu.VMEM((2, half_tp, rows, features), bf16),
+            pltpu.VMEM((2, length, features // 2), bf16),
+            pltpu.VMEM((2, length // 2, features // 2), bf16),
+            pltpu.VMEM((2, length // 2, features // 2), bf16),
+            pltpu.VMEM((2, half_tp, 2, rows, features // 2), bf16),
             dma((2, half_tp)),
             dma((2, half_tp)),
             dma((2, half_tp)),
@@ -759,22 +789,23 @@
             dma((steps,)),
             dma((steps,)),
             dma((steps,)),
-            dma((1,)),
-            dma((1,)),
-            dma((tp,)),
-            dma((2, half_tp)),
+            dma((2,)),
+            dma((2,)),
+            dma((2, tp)),
+            dma((2, half_tp, 2)),
         ],
         compiler_params=pltpu.CompilerParams(collective_id=0, has_side_effects=True),
     )(
         tokens,
-        pre_gain.astype(f32)[None, :],
+        pre_gain,
         w_query,
         w_key,
         w_value,
-        w_igate,
-        w_fgate,
-        base,
-        head_gain.astype(f32)[None, :],
+        w_igate.T,
+        w_fgate.T,
+        forget_bias,
+        gate_drift.T,
+        head_gain,
         w_out,
     )
 

time: 90.4 us -> 81.5 us (0.902)
  the two profiles are of different devices: /device:TPU:13 before, /device:TPU:29 now
where the time goes in v3:
time: 81.5 us; the launch traced here: 81.4 us
  Pallas kernels  79.8 us (98%)
  local copies, waits for them, and re-layouts  1.57 us (2%)
    pallas_call x1, Pallas kernels, on_device_ring(): pl.pallas_call(functools.partial(square_kernel, n, tp), out_shape=jax.Sha...  79.8 us

profile of v3, /device:TPU:29, one launch (start us, length us, event | category | flops | bytes accessed | tf_op | source)
XLA Modules:
  0.0 81.4 jit_solution(13753696505290278432)
XLA Ops:
  0.0 79.8 %shard_map.109 = bf16[32,2048]{1,0:T(8,128)(2,1)} custom-call(bf16[32,2048]{1,0:T(8,128)(2,1)} %tokens.1, bf16[2048]{0:T(1024)(128)(2,1)} %pre_gain.1, bf16[256,256]{1,0:T(8,128)(2,1)} %w_query.1, bf16[256,256]{1,0:T(8,128)(2,1)} %w_key.1, bf16[256,512]{1,0:T(8,128)(2,1)} %w_value.1, bf16[8,2048]{1,0:T(8,128)(2,1)} %bitcast.3, bf16[8,2048]{1,0:T(8,128)(2,1)} %bitcast.4, ...), custom_call_target="tpu_custom_call" | custom-call | tf_op jit(solution)/shard_map/pallas_call | solution.py:754
  79.8 1.6 %copy.13 = bf16[32,2048]{1,0:T(8,128)(2,1)} copy(bf16[32,2048]{1,0:T(8,128)(2,1)} %shard_map.109) | data formatting | bytes 262144

commit v4 on v3

--- a/solution.py
+++ b/solution.py
@@ -280,6 +280,8 @@
     drift_recv,
     near_send,
     near_recv,
+    far_send,
+    far_recv,
     first_sems,
     first_recv,
     ring_send,
@@ -463,61 +465,54 @@
     half_tp = tp // 2
     x = s % 2
     row_at = pl.ds(pl.multiple_of(x * span_rows + t * rows, rows), rows)
+
+    def tokens_at(xx, to_t):
+        start = pl.multiple_of(xx * span_rows + to_t * rows, rows)
+        return tok_all.at[pl.ds(start, rows)]
+
+    for p in range(3):
+        ring_step(p, 0, 0)
     for g in range(2):
-        for yy in range(half_tp):
-            to_s, to_t = g * q + s // 2, 2 * yy + c
-            send_or_keep(
-                tokens,
-                tok_all.at[row_at],
-                tok_send.at[g, yy],
-                tok_recv.at[x, y],
-                to_s,
-                to_t,
-            )
-            send_or_keep(
-                drift,
-                drift_in.at[x, y],
-                drift_send.at[g, yy],
-                drift_recv.at[x, y],
-                to_s,
-                to_t,
-            )
-
-    first_send(3)
-    for k in range(steps):
+        to_s = g * q + s // 2
+        send_or_keep(
+            tokens, tok_all.at[row_at], tok_send.at[g], tok_recv.at[x], to_s, t
+        )
+        send_or_keep(
+            drift, drift_in.at[x], drift_send.at[g], drift_recv.at[x], to_s, t
+        )
+    for k in range(1, steps):
         for p in range(3):
             ring_step(p, 0, k)
+    first_send(3)
     for p in range(3):
         ring_start(p, 1)
-    for k in range(steps - 1):
+    for xx in range(2):
+        block = tokens_at(xx, t)
+        arrived(block, tok_recv.at[xx])
+        arrived(drift_in.at[xx], drift_recv.at[xx])
+        for i in range(1, half_tp):
+            far_t = 2 * lax.rem(y + i, half_tp) + c
+            send(block, block, far_send.at[xx, i - 1], far_recv.at[xx, i - 1], s, far_t)
+        send(block, block, near_send.at[xx, 0], near_recv.at[xx, 0], s, near)
+    for p in range(3):
+        ring_step(p, 1, 0)
+    for xx in range(2):
+        for i in range(1, half_tp):
+            block = tokens_at(xx, 2 * lax.rem(y - i + half_tp, half_tp) + c)
+            arrived(block, far_recv.at[xx, i - 1])
+            send(block, block, near_send.at[xx, i], near_recv.at[xx, i], s, near)
+    for k in range(1, steps - 1):
         for p in range(3):
             ring_step(p, 1, k)
+    ring_start(3, 0)
     for xx in range(2):
-        for yy in range(half_tp):
-            at = pl.ds(
-                pl.multiple_of(xx * span_rows + (2 * yy + c) * rows, rows), rows
-            )
-            arrived(tok_all.at[at], tok_recv.at[xx, yy])
-            arrived(drift_in.at[xx, yy], drift_recv.at[xx, yy])
-            send(
-                tok_all.at[at],
-                tok_all.at[at],
-                near_send.at[xx, yy],
-                near_recv.at[xx, yy],
-                s,
-                near,
-            )
-    for xx in range(2):
-        for yy in range(half_tp):
-            at = pl.ds(
-                pl.multiple_of(xx * span_rows + (2 * yy + 1 - c) * rows, rows), rows
-            )
-            arrived(tok_all.at[at], near_recv.at[xx, yy])
+        for i in range(half_tp):
+            block = tokens_at(xx, 2 * lax.rem(y - i + half_tp, half_tp) + 1 - c)
+            arrived(block, near_recv.at[xx, i])
     wide = tok_all[...].astype(f32)
     scale = lax.rsqrt(jnp.mean(wide * wide, axis=1, keepdims=True) + norm_floor)
     normed[...] = (wide * scale * pre_gain[...].astype(f32)[None, :]).astype(bf16)
 
-    ring_start(3, 0)
     own_product(0, True)
     for k in range(steps):
         step_product(0, k)
@@ -533,7 +528,7 @@
     pick = lax.broadcasted_iota(jnp.int32, gate_in.shape, 1) == head
     late = lax.broadcasted_iota(jnp.int32, (length, 1), 0) >= span_rows
     mine = pl.ds(head, 1)
-    offset = jnp.where(late, drift_in[1, 0, mine, :][:, :1], drift_in[0, 0, mine, :][:, :1])
+    offset = jnp.where(late, drift_in[1, mine, :][:, :1], drift_in[0, mine, :][:, :1])
     forget_pre = (
         jnp.sum(jnp.where(pick, gate_forget, 0.0), axis=1, keepdims=True)
         + forget_bias[head]
@@ -596,10 +591,8 @@
     weights = dot_nt(queries, keys) * decay
     numer = jnp.dot(weights.astype(bf16), values, preferred_element_type=f32)
     denom = jnp.sum(weights, axis=1, keepdims=True)
-    for k in range(1, steps):
-        ring_step(3, 0, k)
-        ring_step(3, 1, k - 1)
-
+    ring_step(3, 0, 1)
+    ring_step(3, 1, 0)
     for pair in state_copies:
         for copy in pair:
             copy.wait_recv()
@@ -684,10 +677,14 @@
 
     share_own(0)
     for k in range(steps):
+        if k > 1:
+            ring_step(3, 0, k)
         share_step(0, k)
     pair = pair_start(0)
     share_own(1)
     for k in range(steps - 1):
+        if k > 0:
+            ring_step(3, 1, k)
         share_step(1, k)
     share_out(0, pair)
     ring_step(3, 1, steps - 1)
@@ -758,7 +755,7 @@
         out_specs=vmem,
         scratch_shapes=[
             pltpu.VMEM((length, width), bf16),
-            pltpu.VMEM((2, half_tp, heads, gate_drift.shape[0]), f32),
+            pltpu.VMEM((2, heads, gate_drift.shape[0]), f32),
             pltpu.VMEM((length, width), bf16),
             *[pltpu.VMEM((2, w.shape[0], w.shape[1] // 2), bf16) for w in weights],
             *[
@@ -775,8 +772,10 @@
             pltpu.VMEM((2, length // 2, features // 2), bf16),
             pltpu.VMEM((2, length // 2, features // 2), bf16),
             pltpu.VMEM((2, half_tp, 2, rows, features // 2), bf16),
-            dma((2, half_tp)),
-            dma((2, half_tp)),
+            dma((2,)),
+            dma((2,)),
+            dma((2,)),
+            dma((2,)),
             dma((2, half_tp)),
             dma((2, half_tp)),
             dma((2, half_tp)),

time: 81.5 us -> 77.1 us (0.946)
  the two profiles are of different devices: /device:TPU:29 before, /device:TPU:13 now
where the time goes in v4:
time: 77.1 us; the launch traced here: 76.9 us
  Pallas kernels  75.4 us (98%)
  local copies, waits for them, and re-layouts  1.57 us (2%)
    pallas_call x1, Pallas kernels, on_device_ring(): pl.pallas_call(functools.partial(square_kernel, n, tp), out_shape=jax.Sha...  75.4 us
    unnamed x1, local copies, waits for them, and re-layouts  1.57 us

profile of v4, /device:TPU:13, one launch (start us, length us, event | category | flops | bytes accessed | tf_op | source)
XLA Modules:
  0.0 76.9 jit_solution(11688018351112408310)
XLA Ops:
  0.0 75.4 %shard_map.109 = bf16[32,2048]{1,0:T(8,128)(2,1)} custom-call(bf16[32,2048]{1,0:T(8,128)(2,1)} %tokens.1, bf16[2048]{0:T(1024)(128)(2,1)} %pre_gain.1, bf16[256,256]{1,0:T(8,128)(2,1)} %w_query.1, bf16[256,256]{1,0:T(8,128)(2,1)} %w_key.1, bf16[256,512]{1,0:T(8,128)(2,1)} %w_value.1, bf16[8,2048]{1,0:T(8,128)(2,1)} %bitcast.3, bf16[8,2048]{1,0:T(8,128)(2,1)} %bitcast.4, ...), custom_call_target="tpu_custom_call" | custom-call | tf_op jit(solution)/shard_map/pallas_call | solution.py:751
  75.4 1.6 %copy.13 = bf16[32,2048]{1,0:T(8,128)(2,1)} copy(bf16[32,2048]{1,0:T(8,128)(2,1)} %shard_map.109) | data formatting | bytes 262144

commit v5 on v4

--- a/solution.py
+++ b/solution.py
@@ -273,6 +273,8 @@
     shares,
     pair_in,
     pair_sum,
+    far_in,
+    final_sum,
     shares_in,
     tok_send,
     tok_recv,
@@ -292,6 +294,8 @@
     aux_recv,
     pair_send,
     pair_recv,
+    sum_send,
+    sum_recv,
     share_send,
     share_recv,
 ):
@@ -516,6 +520,8 @@
     own_product(0, True)
     for k in range(steps):
         step_product(0, k)
+    ring_step(3, 0, 0)
+    ring_start(3, 1)
     own_product(1, False)
     for k in range(steps - 1):
         step_product(1, k)
@@ -548,12 +554,9 @@
     peak = jnp.max(log_pair, axis=1, keepdims=True)
     decay = jnp.where(causal, jnp.exp(log_pair - peak), 0.0)
 
-    ring_step(3, 0, 0)
     for p in range(3):
         ring_step(p, 1, steps - 1)
     step_product(1, steps - 1)
-    ring_start(3, 1)
-
     keys = (acc[:, cols[0]] * (dk**-0.5)).astype(bf16)
     values = acc[:, cols[1]].astype(bf16)
     queries = acc[:, cols[2]].astype(bf16)
@@ -659,20 +662,43 @@
             near,
         )
 
-    def share_out(block, pair):
+    def far_start(block, pair):
         pair.wait_recv()
         pair_sum[block] = (
             shares[block, kept, :].astype(f32) + pair_in[block].astype(f32)
         ).astype(bf16)
+        found = []
+        for i in range(1, half_tp):
+            yy = lax.rem(y + i, half_tp)
+            at = pl.ds(pl.multiple_of(yy * 2 * rows, 2 * rows), 2 * rows)
+            found.append(
+                send(
+                    pair_sum.at[block, at],
+                    far_in.at[block, i - 1],
+                    sum_send.at[block, i - 1],
+                    sum_recv.at[block, i - 1],
+                    s,
+                    2 * yy + c,
+                )
+            )
+        return found
+
+    def share_out(block, found):
+        at = pl.ds(pl.multiple_of(y * 2 * rows, 2 * rows), 2 * rows)
+        total = pair_sum[block, at, :].astype(f32)
+        for i, copy in enumerate(found):
+            copy.wait_recv()
+            total = total + far_in[block, i].astype(f32)
+        final_sum[block] = total.astype(bf16)
         side = zh if block == 0 else 1 - zh
-        for to_t in range(tp):
+        for cc in range(2):
             send_or_keep(
-                pair_sum.at[block, pl.ds(to_t * rows, rows)],
-                shares_in.at[zh, y, side],
-                share_send.at[block, to_t],
-                share_recv.at[zh, y, side],
+                final_sum.at[block, pl.ds(cc * rows, rows)],
+                shares_in.at[zh, side],
+                share_send.at[block, cc],
+                share_recv.at[zh, side],
                 2 * r + c,
-                to_t,
+                2 * y + cc,
             )
 
     share_own(0)
@@ -686,16 +712,18 @@
         if k > 0:
             ring_step(3, 1, k)
         share_step(1, k)
-    share_out(0, pair)
+    found = far_start(0, pair)
     ring_step(3, 1, steps - 1)
     share_step(1, steps - 1)
-    share_out(1, pair_start(1))
+    pair = pair_start(1)
+    share_out(0, found)
+    found = far_start(1, pair)
+    share_out(1, found)
     for side in range(2):
         total = jnp.zeros((rows, wide_half), f32)
         for g in range(2):
-            for yy in range(half_tp):
-                arrived(shares_in.at[g, yy, side], share_recv.at[g, yy, side])
-                total = total + shares_in[g, yy, side].astype(f32)
+            arrived(shares_in.at[g, side], share_recv.at[g, side])
+            total = total + shares_in[g, side].astype(f32)
         out[:, side * wide_half : (side + 1) * wide_half] = total.astype(bf16)
     for copy in copies:
         copy.wait_send()
@@ -771,7 +799,9 @@
             pltpu.VMEM((2, length, features // 2), bf16),
             pltpu.VMEM((2, length // 2, features // 2), bf16),
             pltpu.VMEM((2, length // 2, features // 2), bf16),
-            pltpu.VMEM((2, half_tp, 2, rows, features // 2), bf16),
+            pltpu.VMEM((2, half_tp - 1, 2 * rows, features // 2), bf16),
+            pltpu.VMEM((2, 2 * rows, features // 2), bf16),
+            pltpu.VMEM((2, 2, rows, features // 2), bf16),
             dma((2,)),
             dma((2,)),
             dma((2,)),
@@ -790,8 +820,10 @@
             dma((steps,)),
             dma((2,)),
             dma((2,)),
-            dma((2, tp)),
-            dma((2, half_tp, 2)),
+            dma((2, half_tp)),
+            dma((2, half_tp)),
+            dma((2, 2)),
+            dma((2, 2)),
         ],
         compiler_params=pltpu.CompilerParams(collective_id=0, has_side_effects=True),
     )(
@@ -825,7 +857,7 @@
     )
     out_specs = P(("sp", "tp"), None)
     body = on_device
-    if mesh.shape["sp"] <= ring_limit and mesh.shape["sp"] % 4 == 0 and mesh.shape["tp"] % 2 == 0:
+    if mesh.shape["sp"] <= ring_limit and mesh.shape["sp"] % 4 == 0 and mesh.shape["tp"] % 4 == 0:
         body = functools.partial(on_device_ring, mesh.shape["sp"], mesh.shape["tp"])
     return jax.shard_map(
         body, mesh=mesh, in_specs=in_specs, out_specs=out_specs, check_vma=False

time: 77.1 us -> 73.9 us (0.958)
  the two profiles are of different devices: /device:TPU:13 before, /device:TPU:1 now
where the time goes in v5:
time: 73.9 us; the launch traced here: 73.8 us
  Pallas kernels  72.2 us (98%)
  local copies, waits for them, and re-layouts  1.57 us (2%)
    pallas_call x1, Pallas kernels, on_device_ring(): pl.pallas_call(functools.partial(square_kernel, n, tp), out_shape=jax.Sha...  72.2 us
    unnamed x1, local copies, waits for them, and re-layouts  1.57 us

profile of v5, /device:TPU:1, one launch (start us, length us, event | category | flops | bytes accessed | tf_op | source)
XLA Modules:
  0.0 73.8 jit_solution(204890773730347227)
XLA Ops:
  0.0 72.2 %shard_map.109 = bf16[32,2048]{1,0:T(8,128)(2,1)} custom-call(bf16[32,2048]{1,0:T(8,128)(2,1)} %tokens.1, bf16[2048]{0:T(1024)(128)(2,1)} %pre_gain.1, bf16[256,256]{1,0:T(8,128)(2,1)} %w_query.1, bf16[256,256]{1,0:T(8,128)(2,1)} %w_key.1, bf16[256,512]{1,0:T(8,128)(2,1)} %w_value.1, bf16[8,2048]{1,0:T(8,128)(2,1)} %bitcast.3, bf16[8,2048]{1,0:T(8,128)(2,1)} %bitcast.4, ...), custom_call_target="tpu_custom_call" | custom-call | tf_op jit(solution)/shard_map/pallas_call | solution.py:779
  72.2 1.6 %copy.13 = bf16[32,2048]{1,0:T(8,128)(2,1)} copy(bf16[32,2048]{1,0:T(8,128)(2,1)} %shard_map.109) | data formatting | bytes 262144

commit v6 on v5

--- a/solution.py
+++ b/solution.py
@@ -520,11 +520,10 @@
     own_product(0, True)
     for k in range(steps):
         step_product(0, k)
-    ring_step(3, 0, 0)
-    ring_start(3, 1)
     own_product(1, False)
     for k in range(steps - 1):
         step_product(1, k)
+    ring_step(3, 0, 0)
     all_normed = normed[...]
     gate_in = dot_nt(all_normed, w_igate[...])
     gate_forget = dot_nt(all_normed, w_fgate[...])
@@ -557,6 +556,7 @@
     for p in range(3):
         ring_step(p, 1, steps - 1)
     step_product(1, steps - 1)
+    ring_start(3, 1)
     keys = (acc[:, cols[0]] * (dk**-0.5)).astype(bf16)
     values = acc[:, cols[1]].astype(bf16)
     queries = acc[:, cols[2]].astype(bf16)

time: 73.9 us -> 73 us (0.988)
  the two profiles are of different devices: /device:TPU:1 before, /device:TPU:13 now
where the time goes in v6:
time: 73 us; the launch traced here: 72.3 us
  Pallas kernels  70.8 us (97%)
  local copies, waits for them, and re-layouts  1.57 us (2%)
    pallas_call x1, Pallas kernels, on_device_ring(): pl.pallas_call(functools.partial(square_kernel, n, tp), out_shape=jax.Sha...  70.8 us
    unnamed x1, local copies, waits for them, and re-layouts  1.57 us

profile of v6, /device:TPU:13, one launch (start us, length us, event | category | flops | bytes accessed | tf_op | source)
XLA Modules:
  0.0 72.3 jit_solution(16918521306720113220)
XLA Ops:
  0.0 70.8 %shard_map.109 = bf16[32,2048]{1,0:T(8,128)(2,1)} custom-call(bf16[32,2048]{1,0:T(8,128)(2,1)} %tokens.1, bf16[2048]{0:T(1024)(128)(2,1)} %pre_gain.1, bf16[256,256]{1,0:T(8,128)(2,1)} %w_query.1, bf16[256,256]{1,0:T(8,128)(2,1)} %w_key.1, bf16[256,512]{1,0:T(8,128)(2,1)} %w_value.1, bf16[8,2048]{1,0:T(8,128)(2,1)} %bitcast.3, bf16[8,2048]{1,0:T(8,128)(2,1)} %bitcast.4, ...), custom_call_target="tpu_custom_call" | custom-call | tf_op jit(solution)/shard_map/pallas_call | solution.py:779
  70.8 1.6 %copy.13 = bf16[32,2048]{1,0:T(8,128)(2,1)} copy(bf16[32,2048]{1,0:T(8,128)(2,1)} %shard_map.109) | data formatting | bytes 262144
